TPU v7x, 32 devices: a whole 2x2x4 slice. The times are simulated.
32 devices in a mesh: sp: 8 (over z, x), tp: 4 (over y, core).
Axes of the slice: x: 2, y: 2, z: 4, core: 2. Of those that a mesh axis runs over, the one named last changes fastest.
Arguments:
- tokens: bfloat16 [1536, 2048], P(('sp', 'tp')), may hold values from -7 to 7
- input_norm_gain: float32 [2048], replicated, may hold values from 0.1 to 1.9
- paired_query_weight: bfloat16 [2048, 512], P('sp', 'tp'), may hold values from -16 to 16
- shared_key_weight: bfloat16 [2048, 64], replicated, may hold values from -1 to 1
- shared_value_weight: bfloat16 [2048, 64], replicated, may hold values from -0.125 to 0.125
- recurrent_query_weight: bfloat16 [2048, 1024], P('sp', 'tp'), may hold values from -0.125 to 0.125
- forget_gate_weight: bfloat16 [2048, 1024], P('sp', 'tp'), may hold values from -0.125 to 0.125
- recurrent_value_weight: bfloat16 [2048, 1024], P('sp', 'tp'), may hold values from -0.125 to 0.125
- attention_output_weight: bfloat16 [2048, 512], P('sp', 'tp'), may hold values from -0.15625 to 0.15625
- recurrent_output_weight: bfloat16 [2048, 1024], P('sp', 'tp'), may hold values from -0.15625 to 0.15625
- attention_head_gain: float32 [64], replicated, may hold values from 0.1 to 1.9
- recurrent_head_gain: float32 [128], replicated, may hold values from 0.1 to 1.9
- second_map_weight: float32 [8], P('tp'), may hold values from 0.3 to 0.8
- forget_leak_rate: float32 [1024], P('tp'), may hold values from 2e-05 to 0.05
- extra_log_decay: float32 [1536, 1024], P('sp', 'tp'), may hold values from -1 to 0
- initial_recurrent_state: float32 [8, 128, 128], P('tp'), may hold values from -0.12 to 0.12
Outputs:
- mixer_out: bfloat16 [1536, 2048], P(('sp', 'tp'))
All inputs are finite; a program needn't handle non-finite values.
Results may differ from a plain program's by a relative error of at most 0.014.
Values may be sent and summed in bfloat16 or wider, within the bound.
A program may use at most 128 MiB of HBM per device.

v0:
```python
import functools
import math

import jax
import jax.numpy as jnp
from jax import lax
from jax.experimental import pallas as pl
from jax.experimental.pallas import tpu as pltpu
from jax.sharding import PartitionSpec as P

QK_DIM = 32
HEAD_DIM = 64
RECURRENT_WIDTH = 128
REC_SPAN = 64
KEY_BLOCK = 1536
EPS = 1e-06
MESH = pl.DeviceIdType.MESH
F32, BF16 = jnp.float32, jnp.bfloat16

NN = (((1,), (0,)), ((), ()))
NT = (((1,), (1,)), ((), ()))
TN = (((0,), (0,)), ((), ()))


def dot(a, b, dims=NN, precision=None):
    return lax.dot_general(a, b, dims, preferred_element_type=F32, precision=precision)


def rms(x, gain):
    return x * lax.rsqrt(jnp.mean(x * x, axis=-1, keepdims=True) + EPS) * gain


def loop(lo, hi, body):
    def step(j, carry):
        body(j)
        return carry

    lax.fori_loop(lo, hi, step, 0)


def kernel(
    n, nt,
    tok, gain, wq, wg, wv, wr, woa, wor, wk, wval, again, rgain, mapw, leak, extra, init,
    out,
    gq, gg, gv, gr, goa, gor, nf, kv, pair, pair_d, units, units_d, prefix, pbuf, rbuf,
    ring_send, ring_recv, n_send, n_recv, kv_send, kv_recv, kt_send, kt_recv,
    p_send, p_recv, st_send, st_recv, de_send, de_recv, o_send, o_recv,
):
    s, t = lax.axis_index("sp"), lax.axis_index("tp")
    half = n // 2
    x, z = s % 2, s // 2
    pos = (1 - x) * z + x * (n - 1 - z)

    def at(p):
        p = (p + 2 * n) % n
        hi = p // half
        return (1 - hi) * 2 * p + hi * (2 * (n - 1 - p) + 1)

    ins = (wq, wg, wv, wr, woa, wor)
    bufs = (gq, gg, gv, gr, goa, gor)
    longer = (1, 0, 1, 0, 1, 1)

    def hops(a, d):
        return half if longer[a] == d else half - 1

    def send(a, d, k, first):
        sign = 1 - 2 * d
        owner = s if first else at(pos - sign * k)
        return pltpu.make_async_remote_copy(
            src_ref=ins[a] if first else bufs[a].at[owner],
            dst_ref=bufs[a].at[owner],
            send_sem=ring_send.at[a, d, k],
            recv_sem=ring_recv.at[a, d, k],
            device_id=(at(pos + sign), t),
            device_id_type=MESH,
        )

    def arrival(a, d, k):
        sign = 1 - 2 * d
        slot = bufs[a].at[at(pos - sign * (k + 1))]
        return pltpu.make_async_remote_copy(
            src_ref=slot, dst_ref=slot,
            send_sem=ring_send.at[a, d, k], recv_sem=ring_recv.at[a, d, k],
            device_id=(at(pos - sign), t), device_id_type=MESH,
        )

    def start(group):
        for a in group:
            for d in (0, 1):
                send(a, d, 0, True).start()

    def ring_hop(group, k):
        for a in group:
            for d in (0, 1):
                count = hops(a, d)

                @pl.when(k < count)
                def _():
                    arrival(a, d, k).wait_recv()

                @pl.when(k + 1 < count)
                def _():
                    send(a, d, k + 1, False).start()

    def ring(group, lo, hi):
        if n <= 8:
            for k in range(lo, hi):
                ring_hop(group, k)
        else:
            loop(lo, hi, lambda k: ring_hop(group, k))

    def finish(group):
        for a in group:
            for d in (0, 1):
                send(a, d, 0, True).wait_send()
                loop(1, hops(a, d), lambda k: send(a, d, k, False).wait_send())

    one, two, three = (1, 2), (3, 0), (4, 5)
    cut = [half * i // 4 for i in range(5)]
    barrier = pltpu.get_barrier_semaphore()

    def greet(peer):
        pl.semaphore_signal(barrier, inc=1, device_id=peer, device_id_type=MESH)

    loop(1, n, lambda j: greet(((s + j) % n, t)))
    for j in range(1, nt):
        greet((s, (t + j) % nt))
    pl.semaphore_wait(barrier, n + nt - 2)
    start(one)

    rows = tok.shape[0]
    normed = rms(tok[...].astype(F32), gain[...]).astype(BF16)
    nf[t] = normed

    def tp_peer(j):
        return (t + j) % nt

    def n_copy(j):
        return pltpu.make_async_remote_copy(
            src_ref=nf.at[t], dst_ref=nf.at[t], send_sem=n_send.at[j], recv_sem=n_recv.at[j],
            device_id=(s, tp_peer(j)), device_id_type=MESH,
        )

    def n_in(j):
        slot = nf.at[(t + nt - j) % nt]
        return pltpu.make_async_remote_copy(
            src_ref=slot, dst_ref=slot, send_sem=n_send.at[j], recv_sem=n_recv.at[j],
            device_id=(s, (t + nt - j) % nt), device_id_type=MESH,
        )

    kv[t, s] = jnp.concatenate(
        [dot(normed, wk[...], NT).astype(BF16), dot(normed, wval[...], NT).astype(BF16)], axis=1
    )
    for j in range(1, nt):
        n_copy(j).start()

    def kv_copy(j):
        return pltpu.make_async_remote_copy(
            src_ref=kv.at[t, s], dst_ref=kv.at[t, s],
            send_sem=kv_send.at[j], recv_sem=kv_recv.at[j],
            device_id=((s + j) % n, t), device_id_type=MESH,
        )

    def kv_in(j):
        slot = kv.at[t, (s + n - j) % n]
        return pltpu.make_async_remote_copy(
            src_ref=slot, dst_ref=slot, send_sem=kv_send.at[j], recv_sem=kv_recv.at[j],
            device_id=((s + n - j) % n, t), device_id_type=MESH,
        )

    def kt_copy(j):
        return pltpu.make_async_remote_copy(
            src_ref=kv.at[t], dst_ref=kv.at[t], send_sem=kt_send.at[j], recv_sem=kt_recv.at[j],
            device_id=(s, tp_peer(j)), device_id_type=MESH,
        )

    def kt_in(j):
        slot = kv.at[(t + nt - j) % nt]
        return pltpu.make_async_remote_copy(
            src_ref=slot, dst_ref=slot, send_sem=kt_send.at[j], recv_sem=kt_recv.at[j],
            device_id=(s, (t + nt - j) % nt), device_id_type=MESH,
        )

    loop(1, n, lambda j: kv_copy(j).start())
    for a in range(6):
        bufs[a][s] = ins[a][...]

    ring(one, 0, max(cut[1], 1))
    loop(1, n, lambda j: kv_in(j).wait_recv())
    for j in range(1, nt):
        kt_copy(j).start()
    ring(one, max(cut[1], 1), half - 1)
    start(two)
    for j in range(1, nt):
        n_in(j).wait_recv()
        kt_in(j).wait_recv()
    ring(one, half - 1, half)

    count = nt * rows
    full = nf[...].reshape(count, nf.shape[2])

    def project(buf):
        return dot(full, buf[...].reshape(full.shape[1], buf.shape[2])).astype(BF16)

    gate = project(gg).astype(F32)
    vals = project(gv)
    ring(two, cut[0], cut[1])

    inflow = leak[...] * (1.0 - jax.nn.sigmoid(gate))
    log_decay = jnp.log(1.0 - inflow) + extra[...]
    spans = count // REC_SPAN
    rr = lax.broadcasted_iota(jnp.int32, (REC_SPAN, REC_SPAN), 0)
    cc = lax.broadcasted_iota(jnp.int32, (REC_SPAN, REC_SPAN), 1)
    lower = (rr >= cc).astype(F32)
    running, offsets = [], []
    offset = jnp.zeros((1, log_decay.shape[1]), F32)
    for i in range(spans):
        part = log_decay[i * REC_SPAN : (i + 1) * REC_SPAN]
        run = dot(lower, part, precision=lax.Precision.HIGHEST)
        running.append(run)
        offsets.append(offset)
        offset = offset + run[REC_SPAN - 1 : REC_SPAN]
    total = offset
    w = RECURRENT_WIDTH
    heads = log_decay.shape[1] // w
    befores = [[None] * spans for _ in range(heads)]
    for h in range(heads):
        c = slice(h * w, (h + 1) * w)
        carried = None
        for i in range(spans):
            r = slice(i * REC_SPAN, (i + 1) * REC_SPAN)
            befores[h][i] = carried
            final = running[i][REC_SPAN - 1 : REC_SPAN, c]
            weight = (inflow[r, c] * jnp.exp(final - running[i][:, c])).astype(BF16)
            new = dot(vals[r, c], weight, TN)
            carried = new if carried is None else carried * jnp.exp(final) + new
        pair[x, h] = carried.astype(BF16)
        pair_d[x, h] = jnp.broadcast_to(total[:, c], pair_d.shape[2:])

    mate = s + 1 - 2 * x

    def mate_copy(i, ref):
        return pltpu.make_async_remote_copy(
            src_ref=ref, dst_ref=ref, send_sem=p_send.at[i], recv_sem=p_recv.at[i],
            device_id=(mate, t), device_id_type=MESH,
        )

    def st_pair(j, peer, owner):
        return (
            pltpu.make_async_remote_copy(
                src_ref=units.at[owner], dst_ref=units.at[owner],
                send_sem=st_send.at[j], recv_sem=st_recv.at[j],
                device_id=(2 * peer + x, t), device_id_type=MESH,
            ),
            pltpu.make_async_remote_copy(
                src_ref=units_d.at[owner], dst_ref=units_d.at[owner],
                send_sem=de_send.at[j], recv_sem=de_recv.at[j],
                device_id=(2 * peer + x, t), device_id_type=MESH,
            ),
        )

    def st_start(j):
        for copy in st_pair(j, z + j, z):
            copy.start()

    def st_wait(j):
        for copy in st_pair(j, z - j, z - j):
            copy.wait_recv()

    mate_copy(0, pair.at[x]).start()
    mate_copy(1, pair_d.at[x]).start()
    ring(two, cut[1], cut[2])
    mate_copy(0, pair.at[1 - x]).wait_recv()
    mate_copy(1, pair_d.at[1 - x]).wait_recv()
    units[z] = (
        pair[0, x].astype(F32) * jnp.exp(pair_d[1, x][0:1]) + pair[1, x].astype(F32)
    ).astype(BF16)
    units_d[z] = pair_d[0, x] + pair_d[1, x]
    loop(1, half - z, st_start)
    ring(two, cut[2], half - 1)
    start(three)
    ring(two, half - 1, half)
    queries = project(gq)
    raw = project(gr).astype(F32)

    key_total = kv.shape[0] * kv.shape[1] * kv.shape[2]
    owners = max(1, min(n, KEY_BLOCK // (nt * rows)))
    blocks = n // owners
    scale = 1.0 / math.sqrt(QK_DIM)

    def attend(h, b):
        both = kv[:, pl.ds(b * owners, owners)].reshape(nt * owners * rows, kv.shape[3])
        values = both[:, 2 * QK_DIM :]
        parts = []
        for comp in range(2):
            lo = (2 * h + comp) * QK_DIM
            keys = both[:, comp * QK_DIM : (comp + 1) * QK_DIM]
            scores = dot(queries[:, lo : lo + QK_DIM], keys, NT) * scale
            peak = jnp.max(scores, axis=1, keepdims=True)
            expo = jnp.exp(scores - peak)
            parts += [peak, jnp.sum(expo, axis=1, keepdims=True), dot(expo.astype(BF16), values)]
        return tuple(parts)

    def merge(a, b):
        parts = []
        for comp in range(2):
            pa, ta, wa = a[3 * comp : 3 * comp + 3]
            pb, tb, wb = b[3 * comp : 3 * comp + 3]
            peak = jnp.maximum(pa, pb)
            ea, eb = jnp.exp(pa - peak), jnp.exp(pb - peak)
            parts += [peak, ta * ea + tb * eb, wa * ea + wb * eb]
        return tuple(parts)

    attn_heads = queries.shape[1] // (2 * QK_DIM)
    hidden = []
    for h in range(attn_heads):
        got = attend(h, 0)
        if blocks > 1:
            got = lax.fori_loop(1, blocks, lambda b, g: merge(g, attend(h, b)), got)
        blended = got[2] / got[1] - mapw[h] * (got[5] / got[4])
        hidden.append(rms(blended, again[...]))
        if h == 0:
            ring(three, cut[0], cut[1])
            loop(1, z + 1, st_wait)

            def chain(k, carry):
                return carry * jnp.exp(units_d[k][0:1]) + units[k].astype(F32)

            prefix[x] = lax.fori_loop(0, z, chain, init[x].T).astype(BF16)
            mate_copy(2, prefix.at[x]).start()
    attn_hidden = jnp.concatenate(hidden, axis=1).astype(BF16)
    ring(three, cut[1], cut[2])

    rec_query = raw * jax.nn.sigmoid(raw)
    local, lifted = [], []
    for h in range(heads):
        c = slice(h * RECURRENT_WIDTH, (h + 1) * RECURRENT_WIDTH)
        outs, lifts = [], []
        for i in range(spans):
            r = slice(i * REC_SPAN, (i + 1) * REC_SPAN)
            run = running[i][:, c]
            dq = (rec_query[r, c] * jnp.exp(run)).astype(BF16)
            within = dot(dq, (inflow[r, c] * jnp.exp(-run)).astype(BF16), NT) * lower
            o = dot(within.astype(BF16), vals[r, c])
            if befores[h][i] is not None:
                o = o + dot(dq, befores[h][i].astype(BF16), NT)
            outs.append(o)
            lifts.append(rec_query[r, c] * jnp.exp(offsets[i][:, c] + run))
        local.append(jnp.concatenate(outs, axis=0))
        lifted.append(jnp.concatenate(lifts, axis=0).astype(BF16))

    mate_copy(2, prefix.at[1 - x]).wait_recv()
    rec = []
    for h in range(heads):
        base = prefix[h].astype(F32)
        later = base * jnp.exp(pair_d[0, h][0:1]) + pair[0, h].astype(F32)
        incoming = jnp.where(x == 1, later, base)
        o = local[h] + dot(lifted[h], incoming.astype(BF16), NT)
        rec.append(rms(o, rgain[...]))
    rec_hidden = jnp.concatenate(rec, axis=1).astype(BF16)

    part_width = pbuf.shape[3]

    def o_copy(b, j):
        return pltpu.make_async_remote_copy(
            src_ref=pbuf.at[b, tp_peer(j)], dst_ref=rbuf.at[b, j],
            send_sem=o_send.at[b, j], recv_sem=o_recv.at[b, j],
            device_id=(s, tp_peer(j)), device_id_type=MESH,
        )

    def out_block(b):
        part = dot(attn_hidden, goa[b], NT) + dot(rec_hidden, gor[b], NT)
        pbuf[b] = part.astype(BF16).reshape(nt, rows, part_width)
        for j in range(1, nt):
            o_copy(b, j).start()

    def both_sides(k):
        out_block(at(pos - k - 1))
        out_block(at(pos + k + 1))

    def repeat(lo, hi, body):
        if n <= 8:
            for k in range(lo, hi):
                body(k)
        else:
            loop(lo, hi, body)

    def arrive(k):
        ring_hop(three, k)
        both_sides(k)

    out_block(s)
    repeat(0, cut[2], both_sides)
    repeat(cut[2], half - 1, arrive)
    ring_hop(three, half - 1)
    out_block(at(pos + half))
    for b in range(n):
        acc = pbuf[b, t].astype(F32)
        for j in range(1, nt):
            o_copy(b, j).wait_recv()
            acc = acc + rbuf[b, j].astype(F32)
        out[:, b * part_width : (b + 1) * part_width] = acc.astype(out.dtype)

    finish(one)
    finish(two)
    finish(three)
    for j in range(1, nt):
        n_copy(j).wait_send()
        kt_copy(j).wait_send()
    loop(1, n, lambda j: kv_copy(j).wait_send())

    def st_done(j):
        for copy in st_pair(j, z + j, z):
            copy.wait_send()

    loop(1, half - z, st_done)
    mate_copy(0, pair.at[x]).wait_send()
    mate_copy(1, pair_d.at[x]).wait_send()
    mate_copy(2, prefix.at[x]).wait_send()

    def o_done(b):
        for j in range(1, nt):
            o_copy(b, j).wait_send()

    loop(0, n, o_done)


def solution(mesh):
    n, nt = mesh.shape["sp"], mesh.shape["tp"]

    def body(
        tokens, input_norm_gain, paired_query_weight, shared_key_weight, shared_value_weight,
        recurrent_query_weight, forget_gate_weight, recurrent_value_weight,
        attention_output_weight, recurrent_output_weight, attention_head_gain,
        recurrent_head_gain, second_map_weight, forget_leak_rate, extra_log_decay,
        initial_recurrent_state,
    ):
        rows, width = tokens.shape
        heads = initial_recurrent_state.shape[0]
        weights = (
            paired_query_weight, forget_gate_weight, recurrent_value_weight,
            recurrent_query_weight, attention_output_weight, recurrent_output_weight,
        )
        half = n // 2
        vm = pl.BlockSpec(memory_space=pltpu.VMEM)
        sm = pl.BlockSpec(memory_space=pltpu.SMEM)
        dma = pltpu.SemaphoreType.DMA
        w = RECURRENT_WIDTH
        return pl.pallas_call(
            functools.partial(kernel, n, nt),
            out_shape=jax.ShapeDtypeStruct((rows, width), BF16),
            in_specs=[vm] * 12 + [sm] + [vm] * 3,
            out_specs=vm,
            scratch_shapes=[pltpu.VMEM((n,) + a.shape, BF16) for a in weights]
            + [
                pltpu.VMEM((nt, rows, width), BF16),
                pltpu.VMEM((nt, n, rows, 2 * QK_DIM + HEAD_DIM), BF16),
                pltpu.VMEM((2, heads, w, w), BF16),
                pltpu.VMEM((2, heads, 8, w), F32),
                pltpu.VMEM((half, w, w), BF16),
                pltpu.VMEM((half, 8, w), F32),
                pltpu.VMEM((2, w, w), BF16),
                pltpu.VMEM((n, nt, rows, width // n), BF16),
                pltpu.VMEM((n, nt, rows, width // n), BF16),
                dma((6, 2, half)), dma((6, 2, half)),
                dma((nt,)), dma((nt,)),
                dma((n,)), dma((n,)),
                dma((nt,)), dma((nt,)),
                dma((3,)), dma((3,)),
                dma((half,)), dma((half,)),
                dma((half,)), dma((half,)),
                dma((n, nt)), dma((n, nt)),
            ],
            compiler_params=pltpu.CompilerParams(
                has_side_effects=True, collective_id=0, vmem_limit_bytes=60 * 1024 * 1024
            ),
        )(
            tokens, input_norm_gain[None], *weights, shared_key_weight.T, shared_value_weight.T,
            attention_head_gain[None], recurrent_head_gain[None], second_map_weight,
            forget_leak_rate[None], extra_log_decay, initial_recurrent_state,
        )

    placed = (
        P(("sp", "tp"), None), P(), P("sp", "tp"), P(), P(), P("sp", "tp"), P("sp", "tp"),
        P("sp", "tp"), P("sp", "tp"), P("sp", "tp"), P(), P(), P("tp"), P("tp"),
        P("sp", "tp"), P("tp", None, None),
    )
    return jax.shard_map(
        body, mesh=mesh, in_specs=placed, out_specs=P(("sp", "tp"), None), check_vma=False
    )
```

profile of v0, /device:TPU:0, one launch (start us, length us, event | category | flops | bytes accessed | tf_op | source)
XLA Modules:
  0.0 76.4 jit_solution(16036140480749514381)
XLA Ops:
  0.0 74.8 %shard_map.154 = bf16[48,2048]{1,0:T(8,128)(2,1)} custom-call(bf16[48,2048]{1,0:T(8,128)(2,1)} %tok.1, f32[1,2048]{1,0:T(1,128)} %bitcast.8, bf16[256,128]{1,0:T(8,128)(2,1)} %wq.1, bf16[256,256]{1,0:T(8,128)(2,1)} %wg.1, bf16[256,256]{1,0:T(8,128)(2,1)} %wv.1, bf16[256,256]{1,0:T(8,128)(2,1)} %wr.1, bf16[256,128]{1,0:T(8,128)(2,1)} %woa.1, ...), custom_call_target="tpu_custom_call" | custom-call | tf_op jit(solution)/shard_map/pallas_call | solution.py:449
  74.8 1.6 %copy.18 = bf16[48,2048]{1,0:T(8,128)(2,1)} copy(bf16[48,2048]{1,0:T(8,128)(2,1)} %shard_map.154) | data formatting | bytes 393216
where the time goes:
time: 76.6 us; the launch traced here: 76.4 us
  Pallas kernels  74.8 us (98%)
  local copies, waits for them, and re-layouts  1.62 us (2%)
    pallas_call x1, Pallas kernels, body(): pl.pallas_call(functools.partial(kernel, n, nt), out_shape=jax.ShapeDtype...  74.8 us
    unnamed x1, local copies, waits for them, and re-layouts  1.62 us

commit v1 on v0

v1 whole, which is shorter than its diff:
```python
import functools
import math

import jax
import jax.numpy as jnp
from jax import lax
from jax.experimental import pallas as pl
from jax.experimental.pallas import tpu as pltpu
from jax.sharding import PartitionSpec as P

QK_DIM = 32
HEAD_DIM = 64
RECURRENT_WIDTH = 128
REC_SPAN = 64
KEY_BLOCK = 1536
OUT_WIDTH = 256
LAGS = (1, 3, 5)
EPS = 1e-06
MESH = pl.DeviceIdType.MESH
F32, BF16 = jnp.float32, jnp.bfloat16

NN = (((1,), (0,)), ((), ()))
NT = (((1,), (1,)), ((), ()))
TN = (((0,), (0,)), ((), ()))


def dot(a, b, dims=NN, precision=None):
    return lax.dot_general(a, b, dims, preferred_element_type=F32, precision=precision)


def rms(x, gain):
    return x * lax.rsqrt(jnp.mean(x * x, axis=-1, keepdims=True) + EPS) * gain


def loop(lo, hi, body):
    def step(j, carry):
        body(j)
        return carry

    lax.fori_loop(lo, hi, step, 0)


def kernel(
    n, nt,
    tok, gain, wq, wg, wv, wr, woa, wor, wk, wval, again, rgain, mapw, leak, extra, init,
    out,
    gb, pk, nf, kvb, xb, xs, st, sd, un, ud, pb, db, sb, yr, zb, zr,
    col_send, col_recv, row_send, row_recv, tg_send, tg_recv, kg_send, kg_recv,
    k1_send, k1_recv, x_send, x_recv, un_send, un_recv, ud_send, ud_recv,
    d_send, d_recv, y_send, y_recv, z_send, z_recv,
):
    s, t = lax.axis_index("sp"), lax.axis_index("tp")
    count_p, count_z, count_h = n // 2, n // 4, nt // 2
    small = count_p <= 4
    x, p = s % 2, s // 2
    zl, zh = p % 2, p // 2
    hi, lo = t // 2, t % 2
    zmate, xmate, cmate = s + 2 - 4 * zl, s + 1 - 2 * x, t + 1 - 2 * lo

    def remote(src, dst, send_sem, recv_sem, device):
        return pltpu.make_async_remote_copy(
            src_ref=src, dst_ref=dst, send_sem=send_sem, recv_sem=recv_sem,
            device_id=device, device_id_type=MESH,
        )

    barrier = pltpu.get_barrier_semaphore()

    def greet(peer):
        pl.semaphore_signal(barrier, inc=1, device_id=peer, device_id_type=MESH)

    loop(1, count_p, lambda j: greet((2 * ((p + j) % count_p) + x, t)))
    greet((xmate, t))
    greet((s, cmate))
    for k in range(1, count_h):
        greet((s, (t + 2 * k) % nt))

    rows, width = tok.shape
    part, half, w = wg.shape[0], wg.shape[0] // 2, RECURRENT_WIDTH
    at_v, at_r, at_q, at_a, at_o = part, 2 * part, 3 * part, 3 * part + half, 4 * part
    groups = ((0, at_v), (at_v, at_r), (at_r, at_a), (at_a, 5 * part))

    def split(ref, lo_row):
        mine = pl.ds(pl.multiple_of(zl * w, w), w)
        other = pl.ds(pl.multiple_of((1 - zl) * w, w), w)
        gb[s, lo_row : lo_row + part] = ref[:, mine]
        pk[lo_row : lo_row + part] = ref[:, other]

    def split_narrow(ref, lo_row):
        v = ref[...]
        a = v.shape[1] // 2
        first = jnp.concatenate([v[:half, :a], v[half:, :a]], axis=1)
        second = jnp.concatenate([v[:half, a:], v[half:, a:]], axis=1)
        gb[s, lo_row : lo_row + half] = jnp.where(zl == 0, first, second)
        pk[lo_row : lo_row + half] = jnp.where(zl == 0, second, first)

    split(wg, 0)
    split(wv, at_v)
    split(wr, at_r)
    split_narrow(wq, at_q)
    split_narrow(woa, at_a)
    split(wor, at_o)
    xb[zl] = extra[:, pl.ds(pl.multiple_of(zl * w, w), w)]
    xs[...] = extra[:, pl.ds(pl.multiple_of((1 - zl) * w, w), w)]

    normed = rms(tok[...].astype(F32), gain[...]).astype(BF16)
    nf[zl, t] = normed
    kvb[zl, t, x, zh] = jnp.concatenate(
        [dot(normed, wk[...], NT).astype(BF16), dot(normed, wval[...], NT).astype(BF16)], axis=1
    )
    pl.semaphore_wait(barrier, count_p + count_h)

    class Gather:
        def __init__(self, ref, send, recv):
            self.ref, self.send, self.recv = ref, send, recv

        def slot(self, zz, owner):
            return self.ref.at[zl if zz == 0 else 1 - zl, owner % nt]

        def copy(self, kind, zz, k, owner, device):
            block = self.slot(zz, owner)
            return remote(block, block, self.send.at[kind, zz, k], self.recv.at[kind, zz, k], device)

        def core_out(self, zz, k):
            return self.copy(0, zz, k, t + nt - 2 * k, (s, cmate))

        def core_in(self, zz, k):
            return self.copy(0, zz, k, cmate + nt - 2 * k, (s, cmate))

        def y_out(self, zz, k):
            return self.copy(1, zz, k, t, (s, (t + 2 * k) % nt))

        def y_in(self, zz, k):
            return self.copy(1, zz, k, t + nt - 2 * k, (s, (t + nt - 2 * k) % nt))

        def z_out(self):
            return self.copy(2, 0, 0, t, (zmate, t))

        def z_in(self):
            block = self.slot(1, t)
            return remote(block, block, self.send.at[2, 0, 0], self.recv.at[2, 0, 0], (zmate, t))

        def start(self):
            self.z_out().start()
            for k in range(1, count_h):
                self.y_out(0, k).start()
            self.core_out(0, 0).start()

        def relay_z(self):
            self.z_in().wait_recv()
            for k in range(1, count_h):
                self.y_out(1, k).start()
            self.core_out(1, 0).start()

        def relay_y(self, zz):
            for k in range(1, count_h):
                self.y_in(zz, k).wait_recv()
                self.core_out(zz, k).start()

        def arrive(self):
            for zz in (0, 1):
                for k in range(count_h):
                    self.core_in(zz, k).wait_recv()

        def finish(self):
            self.z_out().wait_send()
            for zz in (0, 1):
                for k in range(count_h):
                    self.core_out(zz, k).wait_send()
                    if k > 0:
                        self.y_out(zz, k).wait_send()

    tokens, keyvals = Gather(nf, tg_send, tg_recv), Gather(kvb, kg_send, kg_recv)

    def cut(ref, g):
        return ref.at[groups[g][0] : groups[g][1]]

    def col_out(p2, g, same):
        return remote(
            cut(gb.at[s], g) if same else cut(pk, g), cut(gb.at[s], g),
            col_send.at[p2, g], col_recv.at[p, g], (2 * p2 + x, t),
        )

    def col_in(p2, g):
        slot = cut(gb.at[2 * p2 + x], g)
        return remote(slot, slot, col_send.at[p2, g], col_recv.at[p2, g], (2 * p2 + x, t))

    def row_out(p2, g):
        slot = cut(gb.at[2 * p2 + x], g)
        return remote(slot, slot, row_send.at[p2, g], row_recv.at[p2, g], (xmate, t))

    def row_in(p2, g):
        slot = cut(gb.at[2 * p2 + 1 - x], g)
        return remote(slot, slot, row_send.at[p2, g], row_recv.at[p2, g], (xmate, t))

    def near(d, body):
        for sign in (1, -1):
            p2 = p + sign * d

            @pl.when((p2 >= 0) & (p2 < count_p))
            def _():
                body(p2)

    def distances(body):
        if small:
            for d in range(1, count_p):
                body(d, d % 2 == 0)
        else:
            loop(0, count_p // 2, lambda i: body(2 * i + 1, False))
            loop(1, count_p // 2, lambda i: body(2 * i, True))

    def issue(g, d):
        if d == 1:
            row_out(p, g).start()
        if small:
            near(d, lambda p2: col_out(p2, g, d % 2 == 0).start())
        elif d == 1:
            distances(lambda e, same: near(e, lambda p2: col_out(p2, g, same).start()))

    def forward_one(g, p2):
        col_in(p2, g).wait_recv()
        row_out(p2, g).start()

    def forward(g, d):
        if small:
            near(d, lambda p2: forward_one(g, p2))
        elif d == 1:
            loop(1, count_p, lambda e: near(e, lambda p2: forward_one(g, p2)))

    def collect(g):
        loop(0, count_p, lambda p2: row_in(p2, g).wait_recv())

    def finish(g):
        distances(lambda d, same: near(d, lambda p2: col_out(p2, g, same).wait_send()))
        loop(0, count_p, lambda p2: row_out(p2, g).wait_send())

    def k1_copy(j, owner):
        block = kvb.at[zl, t, x, owner % count_z]
        peer = (zh + j) % count_z
        return remote(block, block, k1_send.at[j], k1_recv.at[j], (4 * peer + 2 * zl + x, t))

    def swap(i, src, dst, device):
        return remote(src, dst, x_send.at[i], x_recv.at[i], device)

    def kv_swap(side):
        return swap(0, kvb.at[zl, t, side], kvb.at[zl, t, side], (xmate, t))

    def extra_swap(side):
        return swap(1, xs, xb.at[side], (zmate, t))

    def st_swap(side):
        return swap(2, st.at[side], st.at[side], (xmate, t))

    def sd_swap(side):
        return swap(3, sd.at[side], sd.at[side], (xmate, t))

    loop(1, count_z, lambda j: k1_copy(j, zh).start())
    issue(0, 1)
    tokens.start()
    issue(0, 2)
    issue(0, 3)
    for d in (1, 2, 3):
        issue(1, d)
    extra_swap(zl).start()
    forward(0, 1)
    tokens.relay_y(0)
    loop(1, count_z, lambda j: k1_copy(j, zh + count_z - j).wait_recv())
    kv_swap(x).start()
    tokens.relay_z()
    forward(0, 2)
    forward(1, 1)
    kv_swap(1 - x).wait_recv()
    keyvals.start()
    forward(0, 3)
    for d in (1, 2, 3):
        issue(2, d)
    tokens.relay_y(1)
    forward(1, 2)
    forward(1, 3)
    tokens.arrive()
    extra_swap(1 - zl).wait_recv()
    collect(0)

    block = nt * rows
    full = nf[...].reshape(2 * block, width)

    def weight(lo_row):
        return gb[:, lo_row : lo_row + part].reshape(n * part, w)

    def widen(v):
        a = v.shape[2] // 2
        both = jnp.concatenate([v[:, :, :a], v[:, :, a:]], axis=1)
        return both.reshape(both.shape[0] * both.shape[1], a)

    gate = dot(full, weight(0)).astype(BF16).astype(F32)
    forward(2, 1)

    leak_mine = jnp.where(zl == 0, leak[:, :w], leak[:, w:])
    inflow = leak_mine * (1.0 - jax.nn.sigmoid(gate))
    log_decay = jnp.log(1.0 - inflow) + xb[...].reshape(2 * block, w)
    spans = block // REC_SPAN
    rr = lax.broadcasted_iota(jnp.int32, (REC_SPAN, REC_SPAN), 0)
    cc = lax.broadcasted_iota(jnp.int32, (REC_SPAN, REC_SPAN), 1)
    lower = (rr >= cc).astype(F32)
    running, offsets, befores, weighted = [], [], [], []
    for j in (0, 1):
        offset = jnp.zeros((1, w), F32)
        for i in range(spans):
            r = slice(j * block + i * REC_SPAN, j * block + (i + 1) * REC_SPAN)
            run = dot(lower, log_decay[r], precision=lax.Precision.HIGHEST)
            final = run[REC_SPAN - 1 : REC_SPAN]
            running.append(run)
            offsets.append(offset)
            offset = offset + final
            weighted.append((inflow[r] * jnp.exp(final - run)).astype(BF16))
        sd[x, j] = jnp.broadcast_to(offset, sd.shape[2:])
    collect(1)
    vals = dot(full, weight(at_v)).astype(BF16)
    for j in (0, 1):
        carried = None
        for i in range(spans):
            r = slice(j * block + i * REC_SPAN, j * block + (i + 1) * REC_SPAN)
            final = running[j * spans + i][REC_SPAN - 1 : REC_SPAN]
            befores.append(carried)
            new = dot(vals[r], weighted[j * spans + i], TN)
            carried = new if carried is None else carried * jnp.exp(final) + new
        st[x, j] = carried.astype(BF16)
    st_swap(x).start()
    sd_swap(x).start()

    forward(2, 2)

    def advance(carried, sx, j):
        return carried * jnp.exp(sd[sx, j][0:1]) + st[sx, j].astype(F32)

    def un_pair(z2, owner):
        device = (4 * z2 + 2 * zl + x, t)
        return (
            remote(un.at[owner], un.at[owner], un_send.at[z2], un_recv.at[owner], device),
            remote(ud.at[owner], ud.at[owner], ud_send.at[z2], ud_recv.at[owner], device),
        )

    def un_start(z2):
        for copy in un_pair(z2, zh):
            copy.start()

    def un_wait(owner):
        for copy in un_pair(owner, owner):
            copy.wait_recv()

    def join_units():
        st_swap(1 - x).wait_recv()
        sd_swap(1 - x).wait_recv()
        unit = st[0, 0].astype(F32)
        for sx, j in ((1, 0), (0, 1), (1, 1)):
            unit = advance(unit, sx, j)
        un[zh] = unit.astype(BF16)
        ud[zh] = sd[0, 0] + sd[1, 0] + sd[0, 1] + sd[1, 1]
        loop(zh + 1, count_z, un_start)

    def un_done(z2):
        for copy in un_pair(z2, zh):
            copy.wait_send()

    keyvals.relay_z()
    keyvals.relay_y(0)
    for d in (1, 2, 3):
        issue(3, d)
    forward(2, 3)
    keyvals.relay_y(1)
    collect(2)
    keyvals.arrive()

    raw = dot(full, weight(at_r)).astype(BF16).astype(F32)
    queries = dot(full, widen(gb[:, at_q:at_a])).astype(BF16)

    zs = max(1, min(count_z, KEY_BLOCK // (4 * block)))
    blocks = count_z // zs
    scale = 1.0 / math.sqrt(QK_DIM)

    def attend(query, b):
        both = kvb[:, :, :, pl.ds(b * zs, zs)].reshape(4 * zs * block, kvb.shape[5])
        values = both[:, 2 * QK_DIM :]
        parts = []
        for comp in range(2):
            cols = slice(comp * QK_DIM, (comp + 1) * QK_DIM)
            scores = dot(query[:, cols], both[:, cols], NT) * scale
            peak = jnp.max(scores, axis=1, keepdims=True)
            expo = jnp.exp(scores - peak)
            parts += [peak, jnp.sum(expo, axis=1, keepdims=True), dot(expo.astype(BF16), values)]
        return tuple(parts)

    def merge(a, b):
        parts = []
        for comp in range(2):
            pa, ta, wa = a[3 * comp : 3 * comp + 3]
            pc, tc, wc = b[3 * comp : 3 * comp + 3]
            peak = jnp.maximum(pa, pc)
            ea, ec = jnp.exp(pa - peak), jnp.exp(pc - peak)
            parts += [peak, ta * ea + tc * ec, wa * ea + wc * ec]
        return tuple(parts)

    hidden = []
    for j in (0, 1):
        query = queries[j * block : (j + 1) * block]
        got = attend(query, 0)
        if blocks > 1:
            got = lax.fori_loop(1, blocks, lambda b, g: merge(g, attend(query, b)), got)
        blended = got[2] / got[1] - mapw[zl] * (got[5] / got[4])
        hidden.append(rms(blended, again[...]))
        forward(3, 1 + j)
        if j == 0:
            join_units()
    attn_hidden = jnp.concatenate(hidden, axis=0).astype(BF16)

    rec_query = raw * jax.nn.sigmoid(raw)
    local, lifted = [], []
    for j in (0, 1):
        outs, lifts = [], []
        for i in range(spans):
            r = slice(j * block + i * REC_SPAN, j * block + (i + 1) * REC_SPAN)
            run = running[j * spans + i]
            before = befores[j * spans + i]
            dq = (rec_query[r] * jnp.exp(run)).astype(BF16)
            within = dot(dq, (inflow[r] * jnp.exp(-run)).astype(BF16), NT) * lower
            o = dot(within.astype(BF16), vals[r])
            if before is not None:
                o = o + dot(dq, before.astype(BF16), NT)
            outs.append(o)
            lifts.append(rec_query[r] * jnp.exp(offsets[j * spans + i] + run))
        local.append(jnp.concatenate(outs, axis=0))
        lifted.append(jnp.concatenate(lifts, axis=0).astype(BF16))

    loop(0, zh, un_wait)

    def chain(k, carry):
        return carry * jnp.exp(ud[k][0:1]) + un[k].astype(F32)

    base = lax.fori_loop(0, zh, chain, init[zl].T)
    s01 = advance(base, 0, 0)
    s10 = advance(s01, 1, 0)
    s11 = advance(s10, 0, 1)
    incoming = (jnp.where(x == 0, base, s01), jnp.where(x == 0, s10, s11))
    rec = []
    for j in (0, 1):
        o = local[j] + dot(lifted[j], incoming[j].astype(BF16), NT)
        rec.append(rms(o, rgain[...]))
    rec_hidden = jnp.concatenate(rec, axis=0).astype(BF16)
    both_hidden = jnp.concatenate([rec_hidden, attn_hidden], axis=1)

    per = pb.shape[5] // part
    fw = per * part
    chunks = n // per

    def d_copy(ch):
        return remote(pb.at[ch, 1 - lo], db.at[ch], d_send.at[ch], d_recv.at[ch], (s, cmate))

    def y_copy(ch, k, flip):
        h2 = (hi + k) % count_h
        src = zb.at[ch, pl.ds(h2, 1)] if flip else sb.at[ch, pl.ds(2 * h2, 2)]
        dst = yr.at[ch, k, pl.ds(0, 1)] if flip else yr.at[ch, k]
        return remote(src, dst, y_send.at[ch, k], y_recv.at[ch, k], (s, 2 * h2 + lo))

    def z_copy(ch, flip):
        src = sb.at[ch, pl.ds(count_h * (1 - zl), count_h)] if flip else zb.at[ch, pl.ds(1 - zl, 1)]
        dst = zr.at[ch] if flip else zr.at[ch, pl.ds(0, 1)]
        return remote(src, dst, z_send.at[ch], z_recv.at[ch], (zmate, t))

    def stage_d(ch):
        shard = gb[pl.ds(ch * per, per)]
        weights = jnp.concatenate(
            [shard[:, at_o:].reshape(fw, w), widen(shard[:, at_a:at_o])], axis=1
        )
        got = dot(both_hidden, weights, NT).astype(BF16)
        for z2 in (0, 1):
            for t2 in range(nt):
                lo_row = (z2 * nt + t2) * rows
                pb[ch, t2 % 2, z2, t2 // 2] = got[lo_row : lo_row + rows]
        d_copy(ch).start()

    def stage_first(ch, flip):
        d_copy(ch).wait_recv()
        total = (pb[ch, lo].astype(F32) + db[ch].astype(F32)).astype(BF16)
        if flip:
            sb[ch] = total.reshape(sb.shape[1:])
            z_copy(ch, flip).start()
        else:
            for h2 in range(count_h):
                sb[ch, 2 * h2 : 2 * h2 + 2] = total[:, h2]
            for k in range(1, count_h):
                y_copy(ch, k, flip).start()

    def stage_second(ch, flip):
        if flip:
            z_copy(ch, flip).wait_recv()
            mine = sb[ch, pl.ds(count_h * zl, count_h)]
            zb[ch] = (mine.astype(F32) + zr[ch].astype(F32)).astype(BF16)
            for k in range(1, count_h):
                y_copy(ch, k, flip).start()
        else:
            total = sb[ch, pl.ds(2 * hi, 2)].astype(F32)
            for k in range(1, count_h):
                y_copy(ch, k, flip).wait_recv()
                total = total + yr[ch, k].astype(F32)
            zb[ch, 0:2] = total.astype(BF16)
            z_copy(ch, flip).start()

    def stage_out(ch, flip):
        if flip:
            total = zb[ch, hi].astype(F32)
            for k in range(1, count_h):
                y_copy(ch, k, flip).wait_recv()
                total = total + yr[ch, k, 0].astype(F32)
        else:
            z_copy(ch, flip).wait_recv()
            total = zb[ch, zl].astype(F32) + zr[ch, 0].astype(F32)
        out[:, pl.ds(pl.multiple_of(ch * fw, fw), fw)] = total.astype(out.dtype)

    if small and per == 1:
        order = []
        for k in range(count_z):
            z2 = (zh + k) % count_z
            pair = (2 * z2, 2 * z2 + 1)
            order += [(q, c) for c in (0, 1) for q in pair] if k == 0 else [(q, c) for q in pair for c in (0, 1)]
        forward(3, 3)
        ready = []
        for q, c in order:
            ready.append((2 * q + x if c == 0 else 2 * q + 1 - x, q if c == 1 else None))
    else:
        collect(3)
        ready = [(ch, None) for ch in range(chunks)]

    lag = len(ready)
    for i in range(lag + LAGS[2]):
        if i < lag:
            ch, q = ready[i]
            if q is not None:
                row_in(q, 3).wait_recv()
            stage_d(ch)
        for body, late in zip((stage_first, stage_second, stage_out), LAGS):
            if 0 <= i - late < lag:
                body(ready[i - late][0], (i - late) % 2 == 1)

    for g in (0, 1, 2, 3):
        finish(g)
    tokens.finish()
    keyvals.finish()
    loop(1, count_z, lambda j: k1_copy(j, zh).wait_send())
    kv_swap(x).wait_send()
    extra_swap(zl).wait_send()
    st_swap(x).wait_send()
    sd_swap(x).wait_send()
    loop(zh + 1, count_z, un_done)

    for i, (ch, _) in enumerate(ready):
        d_copy(ch).wait_send()
        for k in range(1, count_h):
            y_copy(ch, k, i % 2 == 1).wait_send()
        z_copy(ch, i % 2 == 1).wait_send()


def solution(mesh):
    n, nt = mesh.shape["sp"], mesh.shape["tp"]

    def body(
        tokens, input_norm_gain, paired_query_weight, shared_key_weight, shared_value_weight,
        recurrent_query_weight, forget_gate_weight, recurrent_value_weight,
        attention_output_weight, recurrent_output_weight, attention_head_gain,
        recurrent_head_gain, second_map_weight, forget_leak_rate, extra_log_decay,
        initial_recurrent_state,
    ):
        rows, width = tokens.shape
        weights = (
            paired_query_weight, forget_gate_weight, recurrent_value_weight,
            recurrent_query_weight, attention_output_weight, recurrent_output_weight,
        )
        part = forget_gate_weight.shape[0]
        span = extra_log_decay.shape[0]
        count_p, count_z, count_h = n // 2, n // 4, nt // 2
        fw = part * max(1, OUT_WIDTH // part)
        chunks = width // fw
        kv_width = 2 * QK_DIM + HEAD_DIM
        vm = pl.BlockSpec(memory_space=pltpu.VMEM)
        sm = pl.BlockSpec(memory_space=pltpu.SMEM)
        dma = pltpu.SemaphoreType.DMA
        w = RECURRENT_WIDTH
        return pl.pallas_call(
            functools.partial(kernel, n, nt),
            out_shape=jax.ShapeDtypeStruct((rows, width), BF16),
            in_specs=[vm] * 12 + [sm] + [vm] * 3,
            out_specs=vm,
            scratch_shapes=[
                pltpu.VMEM((n, 5 * part, w), BF16),
                pltpu.VMEM((5 * part, w), BF16),
                pltpu.VMEM((2, nt, rows, width), BF16),
                pltpu.VMEM((2, nt, 2, count_z, rows, kv_width), BF16),
                pltpu.VMEM((2, span, w), F32),
                pltpu.VMEM((span, w), F32),
                pltpu.VMEM((2, 2, w, w), BF16),
                pltpu.VMEM((2, 2, 8, w), F32),
                pltpu.VMEM((count_z, w, w), BF16),
                pltpu.VMEM((count_z, 8, w), F32),
                pltpu.VMEM((chunks, 2, 2, count_h, rows, fw), BF16),
                pltpu.VMEM((chunks, 2, count_h, rows, fw), BF16),
                pltpu.VMEM((chunks, 2 * count_h, rows, fw), BF16),
                pltpu.VMEM((chunks, count_h, 2, rows, fw), BF16),
                pltpu.VMEM((chunks, max(2, count_h), rows, fw), BF16),
                pltpu.VMEM((chunks, max(2, count_h), rows, fw), BF16),
                dma((count_p, 4)), dma((count_p, 4)),
                dma((count_p, 4)), dma((count_p, 4)),
                dma((3, 2, count_h)), dma((3, 2, count_h)),
                dma((3, 2, count_h)), dma((3, 2, count_h)),
                dma((count_z,)), dma((count_z,)),
                dma((4,)), dma((4,)),
                dma((count_z,)), dma((count_z,)),
                dma((count_z,)), dma((count_z,)),
                dma((chunks,)), dma((chunks,)),
                dma((chunks, count_h)), dma((chunks, count_h)),
                dma((chunks,)), dma((chunks,)),
            ],
            compiler_params=pltpu.CompilerParams(
                has_side_effects=True, collective_id=0, vmem_limit_bytes=60 * 1024 * 1024
            ),
        )(
            tokens, input_norm_gain[None], *weights, shared_key_weight.T, shared_value_weight.T,
            attention_head_gain[None], recurrent_head_gain[None], second_map_weight,
            forget_leak_rate[None], extra_log_decay, initial_recurrent_state,
        )

    placed = (
        P(("sp", "tp"), None), P(), P("sp", "tp"), P(), P(), P("sp", "tp"), P("sp", "tp"),
        P("sp", "tp"), P("sp", "tp"), P("sp", "tp"), P(), P(), P("tp"), P("tp"),
        P("sp", "tp"), P("tp", None, None),
    )
    return jax.shard_map(
        body, mesh=mesh, in_specs=placed, out_specs=P(("sp", "tp"), None), check_vma=False
    )
```

time: 76.6 us -> 64.6 us (0.84)
  Pallas kernels: 74.8 us -> 62.8 us
    pallas_call x1, Pallas kernels: 74.8 us -> 62.8 us  [body(): pl.pallas_call(functools.partial(kernel, n, nt), out_shape=jax.ShapeDtype...]
where the time goes in v1:
time: 64.6 us; the launch traced here: 64.5 us
  Pallas kernels  62.8 us (97%)
  local copies, waits for them, and re-layouts  1.62 us (3%)
    pallas_call x1, Pallas kernels, body(): pl.pallas_call(functools.partial(kernel, n, nt), out_shape=jax.ShapeDtype...  62.8 us
    unnamed x1, local copies, waits for them, and re-layouts  1.62 us

profile of v1, /device:TPU:0, one launch (start us, length us, event | category | flops | bytes accessed | tf_op | source)
XLA Modules:
  0.0 64.5 jit_solution(11803788149116475070)
XLA Ops:
  0.0 62.8 %shard_map.154 = bf16[48,2048]{1,0:T(8,128)(2,1)} custom-call(bf16[48,2048]{1,0:T(8,128)(2,1)} %tok.1, f32[1,2048]{1,0:T(1,128)} %bitcast.8, bf16[256,128]{1,0:T(8,128)(2,1)} %wq.1, bf16[256,256]{1,0:T(8,128)(2,1)} %wg.1, bf16[256,256]{1,0:T(8,128)(2,1)} %wv.1, bf16[256,256]{1,0:T(8,128)(2,1)} %wr.1, bf16[256,128]{1,0:T(8,128)(2,1)} %woa.1, ...), custom_call_target="tpu_custom_call" | custom-call | tf_op jit(solution)/shard_map/pallas_call | solution.py:586
  62.8 1.6 %copy.18 = bf16[48,2048]{1,0:T(8,128)(2,1)} copy(bf16[48,2048]{1,0:T(8,128)(2,1)} %shard_map.154) | data formatting | bytes 393216

commit v2 on v1

--- a/solution.py
+++ b/solution.py
@@ -14,7 +14,7 @@
 REC_SPAN = 64
 KEY_BLOCK = 1536
 OUT_WIDTH = 256
-LAGS = (1, 3, 5)
+LAGS = (2, 5, 8)
 EPS = 1e-06
 MESH = pl.DeviceIdType.MESH
 F32, BF16 = jnp.float32, jnp.bfloat16
@@ -42,8 +42,10 @@
 
 def kernel(
     n, nt,
-    tok, gain, wq, wg, wv, wr, woa, wor, wk, wval, again, rgain, mapw, leak, extra, init,
-    out,
+    tok_in, gain, wq_in, wg_in, wv_in, wr_in, woa_in, wor_in, wk_in, wval_in, again, rgain, mapw, leak,
+    extra_in, init_in,
+    out_ref,
+    tok, wq, wg, wv, wr, woa, wor, wk, wval, extra, init, out, in_sem, out_sem,
     gb, pk, nf, kvb, xb, xs, st, sd, un, ud, pb, db, sb, yr, zb, zr,
     col_send, col_recv, row_send, row_recv, tg_send, tg_recv, kg_send, kg_recv,
     k1_send, k1_recv, x_send, x_recv, un_send, un_recv, ud_send, ud_recv,
@@ -63,6 +65,13 @@
             device_id=device, device_id_type=MESH,
         )
 
+    order_in = (
+        (tok_in, tok), (wg_in, wg), (wv_in, wv), (wq_in, wq), (wr_in, wr), (woa_in, woa),
+        (wor_in, wor), (extra_in, extra), (wk_in, wk), (wval_in, wval), (init_in, init),
+    )
+    loads = [pltpu.make_async_copy(a, b, in_sem.at[i]) for i, (a, b) in enumerate(order_in)]
+    for load in loads:
+        load.start()
     barrier = pltpu.get_barrier_semaphore()
 
     def greet(peer):
@@ -74,9 +83,12 @@
     for k in range(1, count_h):
         greet((s, (t + 2 * k) % nt))
 
+    for load in loads:
+        load.wait()
+
     rows, width = tok.shape
     part, half, w = wg.shape[0], wg.shape[0] // 2, RECURRENT_WIDTH
-    at_v, at_r, at_q, at_a, at_o = part, 2 * part, 3 * part, 3 * part + half, 4 * part
+    at_v, at_q, at_r, at_a, at_o = part, 2 * part, 2 * part + half, 3 * part + half, 4 * part
     groups = ((0, at_v), (at_v, at_r), (at_r, at_a), (at_a, 5 * part))
 
     def split(ref, lo_row):
@@ -99,8 +111,7 @@
     split_narrow(wq, at_q)
     split_narrow(woa, at_a)
     split(wor, at_o)
-    xb[zl] = extra[:, pl.ds(pl.multiple_of(zl * w, w), w)]
-    xs[...] = extra[:, pl.ds(pl.multiple_of((1 - zl) * w, w), w)]
+    xs[...] = extra[:, pl.ds(pl.multiple_of((1 - zl) * w, w), w)].astype(BF16)
 
     normed = rms(tok[...].astype(F32), gain[...]).astype(BF16)
     nf[zl, t] = normed
@@ -208,23 +219,32 @@
             loop(0, count_p // 2, lambda i: body(2 * i + 1, False))
             loop(1, count_p // 2, lambda i: body(2 * i, True))
 
-    def issue(g, d):
-        if d == 1:
-            row_out(p, g).start()
-        if small:
-            near(d, lambda p2: col_out(p2, g, d % 2 == 0).start())
-        elif d == 1:
-            distances(lambda e, same: near(e, lambda p2: col_out(p2, g, same).start()))
+    def columns(g):
+        distances(lambda d, same: near(d, lambda p2: col_out(p2, g, same).start()))
+
+    sources = (count_z - zh, p + 1 - 2 * zl, (count_p - 1) * (1 - zh))
 
     def forward_one(g, p2):
         col_in(p2, g).wait_recv()
         row_out(p2, g).start()
 
-    def forward(g, d):
+    def forward(g, i):
         if small:
-            near(d, lambda p2: forward_one(g, p2))
-        elif d == 1:
+            forward_one(g, sources[i])
+        elif i == 0:
             loop(1, count_p, lambda e: near(e, lambda p2: forward_one(g, p2)))
+
+    at_edge = (p == 0) | (p == count_p - 1)
+
+    def at_end(body):
+        if small:
+            pl.when(at_edge)(body)
+
+    def at_middle(body):
+        if small:
+            pl.when(jnp.logical_not(at_edge))(body)
+        else:
+            body()
 
     def collect(g):
         loop(0, count_p, lambda p2: row_in(p2, g).wait_recv())
@@ -244,8 +264,8 @@
     def kv_swap(side):
         return swap(0, kvb.at[zl, t, side], kvb.at[zl, t, side], (xmate, t))
 
-    def extra_swap(side):
-        return swap(1, xs, xb.at[side], (zmate, t))
+    def extra_swap():
+        return swap(1, xs, xb, (zmate, t))
 
     def st_swap(side):
         return swap(2, st.at[side], st.at[side], (xmate, t))
@@ -254,30 +274,36 @@
         return swap(3, sd.at[side], sd.at[side], (xmate, t))
 
     loop(1, count_z, lambda j: k1_copy(j, zh).start())
-    issue(0, 1)
     tokens.start()
-    issue(0, 2)
-    issue(0, 3)
-    for d in (1, 2, 3):
-        issue(1, d)
-    extra_swap(zl).start()
-    forward(0, 1)
-    tokens.relay_y(0)
+    row_out(p, 0).start()
+    row_out(p, 1).start()
+    columns(0)
+    columns(1)
+    extra_swap().start()
     loop(1, count_z, lambda j: k1_copy(j, zh + count_z - j).wait_recv())
     kv_swap(x).start()
+    row_out(p, 2).start()
+    row_out(p, 3).start()
+    forward(0, 0)
+    kv_swap(1 - x).wait_recv()
+    keyvals.start()
+    columns(2)
+    tokens.relay_y(0)
     tokens.relay_z()
+    at_middle(lambda: forward(1, 0))
+    forward(0, 1)
     forward(0, 2)
     forward(1, 1)
-    kv_swap(1 - x).wait_recv()
-    keyvals.start()
-    forward(0, 3)
-    for d in (1, 2, 3):
-        issue(2, d)
+    at_end(lambda: forward(1, 0))
     tokens.relay_y(1)
     forward(1, 2)
-    forward(1, 3)
+    columns(3)
+    keyvals.relay_z()
+    keyvals.relay_y(0)
+    at_middle(lambda: forward(2, 0))
+    at_middle(lambda: forward(2, 1))
     tokens.arrive()
-    extra_swap(1 - zl).wait_recv()
+    extra_swap().wait_recv()
     collect(0)
 
     block = nt * rows
@@ -292,11 +318,12 @@
         return both.reshape(both.shape[0] * both.shape[1], a)
 
     gate = dot(full, weight(0)).astype(BF16).astype(F32)
-    forward(2, 1)
-
     leak_mine = jnp.where(zl == 0, leak[:, :w], leak[:, w:])
     inflow = leak_mine * (1.0 - jax.nn.sigmoid(gate))
-    log_decay = jnp.log(1.0 - inflow) + xb[...].reshape(2 * block, w)
+    here = extra[:, pl.ds(pl.multiple_of(zl * w, w), w)]
+    there = xb[...].astype(F32)
+    added = jnp.concatenate([jnp.where(zl == 0, here, there), jnp.where(zl == 0, there, here)], axis=0)
+    log_decay = jnp.log(1.0 - inflow) + added
     spans = block // REC_SPAN
     rr = lax.broadcasted_iota(jnp.int32, (REC_SPAN, REC_SPAN), 0)
     cc = lax.broadcasted_iota(jnp.int32, (REC_SPAN, REC_SPAN), 1)
@@ -313,8 +340,12 @@
             offset = offset + final
             weighted.append((inflow[r] * jnp.exp(final - run)).astype(BF16))
         sd[x, j] = jnp.broadcast_to(offset, sd.shape[2:])
+    at_end(lambda: forward(2, 1))
+    forward(2, 2)
+    at_end(lambda: forward(2, 0))
     collect(1)
-    vals = dot(full, weight(at_v)).astype(BF16)
+    both = dot(full, jnp.concatenate([weight(at_v), widen(gb[:, at_q:at_r])], axis=1)).astype(BF16)
+    vals, queries = both[:, :w], both[:, w:]
     for j in (0, 1):
         carried = None
         for i in range(spans):
@@ -327,7 +358,6 @@
     st_swap(x).start()
     sd_swap(x).start()
 
-    forward(2, 2)
 
     def advance(carried, sx, j):
         return carried * jnp.exp(sd[sx, j][0:1]) + st[sx, j].astype(F32)
@@ -361,21 +391,13 @@
         for copy in un_pair(z2, zh):
             copy.wait_send()
 
-    keyvals.relay_z()
-    keyvals.relay_y(0)
-    for d in (1, 2, 3):
-        issue(3, d)
-    forward(2, 3)
     keyvals.relay_y(1)
-    collect(2)
     keyvals.arrive()
 
-    raw = dot(full, weight(at_r)).astype(BF16).astype(F32)
-    queries = dot(full, widen(gb[:, at_q:at_a])).astype(BF16)
-
+    forward(3, 1)
     zs = max(1, min(count_z, KEY_BLOCK // (4 * block)))
     blocks = count_z // zs
-    scale = 1.0 / math.sqrt(QK_DIM)
+    scale = math.log2(math.e) / math.sqrt(QK_DIM)
 
     def attend(query, b):
         both = kvb[:, :, :, pl.ds(b * zs, zs)].reshape(4 * zs * block, kvb.shape[5])
@@ -383,9 +405,9 @@
         parts = []
         for comp in range(2):
             cols = slice(comp * QK_DIM, (comp + 1) * QK_DIM)
-            scores = dot(query[:, cols], both[:, cols], NT) * scale
+            scores = dot(query[:, cols], both[:, cols], NT)
             peak = jnp.max(scores, axis=1, keepdims=True)
-            expo = jnp.exp(scores - peak)
+            expo = jnp.exp2((scores - peak) * scale)
             parts += [peak, jnp.sum(expo, axis=1, keepdims=True), dot(expo.astype(BF16), values)]
         return tuple(parts)
 
@@ -395,7 +417,7 @@
             pa, ta, wa = a[3 * comp : 3 * comp + 3]
             pc, tc, wc = b[3 * comp : 3 * comp + 3]
             peak = jnp.maximum(pa, pc)
-            ea, ec = jnp.exp(pa - peak), jnp.exp(pc - peak)
+            ea, ec = jnp.exp2((pa - peak) * scale), jnp.exp2((pc - peak) * scale)
             parts += [peak, ta * ea + tc * ec, wa * ea + wc * ec]
         return tuple(parts)
 
@@ -407,11 +429,12 @@
             got = lax.fori_loop(1, blocks, lambda b, g: merge(g, attend(query, b)), got)
         blended = got[2] / got[1] - mapw[zl] * (got[5] / got[4])
         hidden.append(rms(blended, again[...]))
-        forward(3, 1 + j)
-        if j == 0:
-            join_units()
     attn_hidden = jnp.concatenate(hidden, axis=0).astype(BF16)
 
+    join_units()
+    forward(3, 2)
+    collect(2)
+    raw = dot(full, weight(at_r)).astype(BF16).astype(F32)
     rec_query = raw * jax.nn.sigmoid(raw)
     local, lifted = [], []
     for j in (0, 1):
@@ -430,6 +453,7 @@
         local.append(jnp.concatenate(outs, axis=0))
         lifted.append(jnp.concatenate(lifts, axis=0).astype(BF16))
 
+    forward(3, 0)
     loop(0, zh, un_wait)
 
     def chain(k, carry):
@@ -514,14 +538,15 @@
             z_copy(ch, flip).wait_recv()
             total = zb[ch, zl].astype(F32) + zr[ch, 0].astype(F32)
         out[:, pl.ds(pl.multiple_of(ch * fw, fw), fw)] = total.astype(out.dtype)
+        store(ch).start()
+
+    def store(ch):
+        cols = pl.ds(pl.multiple_of(ch * fw, fw), fw)
+        return pltpu.make_async_copy(out.at[:, cols], out_ref.at[:, cols], out_sem.at[ch])
 
     if small and per == 1:
-        order = []
-        for k in range(count_z):
-            z2 = (zh + k) % count_z
-            pair = (2 * z2, 2 * z2 + 1)
-            order += [(q, c) for c in (0, 1) for q in pair] if k == 0 else [(q, c) for q in pair for c in (0, 1)]
-        forward(3, 3)
+        order = [(q, c) for c in (0, 1) for q in (2 * zh, 2 * zh + 1)]
+        order += [(q, c) for q in (sources[2], sources[0]) for c in (0, 1)]
         ready = []
         for q, c in order:
             ready.append((2 * q + x if c == 0 else 2 * q + 1 - x, q if c == 1 else None))
@@ -546,7 +571,7 @@
     keyvals.finish()
     loop(1, count_z, lambda j: k1_copy(j, zh).wait_send())
     kv_swap(x).wait_send()
-    extra_swap(zl).wait_send()
+    extra_swap().wait_send()
     st_swap(x).wait_send()
     sd_swap(x).wait_send()
     loop(zh + 1, count_z, un_done)
@@ -556,6 +581,7 @@
         for k in range(1, count_h):
             y_copy(ch, k, i % 2 == 1).wait_send()
         z_copy(ch, i % 2 == 1).wait_send()
+        store(ch).wait()
 
 
 def solution(mesh):
@@ -579,6 +605,9 @@
         fw = part * max(1, OUT_WIDTH // part)
         chunks = width // fw
         kv_width = 2 * QK_DIM + HEAD_DIM
+        wk, wval = shared_key_weight.T, shared_value_weight.T
+        staged = (tokens, *weights, wk, wval, extra_log_decay, initial_recurrent_state)
+        hb = pl.BlockSpec(memory_space=pl.ANY)
         vm = pl.BlockSpec(memory_space=pltpu.VMEM)
         sm = pl.BlockSpec(memory_space=pltpu.SMEM)
         dma = pltpu.SemaphoreType.DMA
@@ -586,15 +615,17 @@
         return pl.pallas_call(
             functools.partial(kernel, n, nt),
             out_shape=jax.ShapeDtypeStruct((rows, width), BF16),
-            in_specs=[vm] * 12 + [sm] + [vm] * 3,
-            out_specs=vm,
-            scratch_shapes=[
+            in_specs=[hb, vm] + [hb] * 8 + [vm] * 2 + [sm, vm, hb, hb],
+            out_specs=hb,
+            scratch_shapes=[pltpu.VMEM(a.shape, a.dtype) for a in staged] + [
+                pltpu.VMEM((rows, width), BF16),
+                dma((len(staged),)), dma((chunks,)),
                 pltpu.VMEM((n, 5 * part, w), BF16),
                 pltpu.VMEM((5 * part, w), BF16),
                 pltpu.VMEM((2, nt, rows, width), BF16),
                 pltpu.VMEM((2, nt, 2, count_z, rows, kv_width), BF16),
-                pltpu.VMEM((2, span, w), F32),
-                pltpu.VMEM((span, w), F32),
+                pltpu.VMEM((span, w), BF16),
+                pltpu.VMEM((span, w), BF16),
                 pltpu.VMEM((2, 2, w, w), BF16),
                 pltpu.VMEM((2, 2, 8, w), F32),
                 pltpu.VMEM((count_z, w, w), BF16),
@@ -621,7 +652,7 @@
                 has_side_effects=True, collective_id=0, vmem_limit_bytes=60 * 1024 * 1024
             ),
         )(
-            tokens, input_norm_gain[None], *weights, shared_key_weight.T, shared_value_weight.T,
+            tokens, input_norm_gain[None], *weights, wk, wval,
             attention_head_gain[None], recurrent_head_gain[None], second_map_weight,
             forget_leak_rate[None], extra_log_decay, initial_recurrent_state,
         )

time: 64.6 us -> 57.3 us (0.89)
  Pallas kernels: 62.8 us -> 55.5 us
    pallas_call x1, Pallas kernels: 62.8 us -> 55.5 us  [body(): pl.pallas_call(functools.partial(kernel, n, nt), out_shape=jax.ShapeDtype...]
where the time goes in v2:
time: 57.3 us; the launch traced here: 57.1 us
  Pallas kernels  55.5 us (97%)
  local copies, waits for them, and re-layouts  1.62 us (3%)
    pallas_call x1, Pallas kernels, body(): pl.pallas_call(functools.partial(kernel, n, nt), out_shape=jax.ShapeDtype...  55.5 us
    unnamed x1, local copies, waits for them, and re-layouts  1.62 us

profile of v2, /device:TPU:0, one launch (start us, length us, event | category | flops | bytes accessed | tf_op | source)
XLA Modules:
  0.0 57.1 jit_solution(5130255474698653778)
XLA Ops:
  0.0 55.5 %shard_map.154 = bf16[48,2048]{1,0:T(8,128)(2,1)} custom-call(bf16[48,2048]{1,0:T(8,128)(2,1)} %tok_in.1, f32[1,2048]{1,0:T(1,128)} %bitcast.8, bf16[256,128]{1,0:T(8,128)(2,1)} %wq_in.1, bf16[256,256]{1,0:T(8,128)(2,1)} %wg_in.1, bf16[256,256]{1,0:T(8,128)(2,1)} %wv_in.1, bf16[256,256]{1,0:T(8,128)(2,1)} %wr_in.1, bf16[256,128]{1,0:T(8,128)(2,1)} %woa_in.1, ...), custom_call_target="tpu_custom_call" | custom-call | tf_op jit(solution)/shard_map/pallas_call | solution.py:615
  55.5 1.6 %copy.18 = bf16[48,2048]{1,0:T(8,128)(2,1)} copy(bf16[48,2048]{1,0:T(8,128)(2,1)} %shard_map.154) | data formatting | bytes 393216

commit v3 on v2

--- a/solution.py
+++ b/solution.py
@@ -14,7 +14,7 @@
 REC_SPAN = 64
 KEY_BLOCK = 1536
 OUT_WIDTH = 256
-LAGS = (2, 5, 8)
+LAGS = (2, 8, 14)
 EPS = 1e-06
 MESH = pl.DeviceIdType.MESH
 F32, BF16 = jnp.float32, jnp.bfloat16
@@ -66,8 +66,8 @@
         )
 
     order_in = (
-        (tok_in, tok), (wg_in, wg), (wv_in, wv), (wq_in, wq), (wr_in, wr), (woa_in, woa),
-        (wor_in, wor), (extra_in, extra), (wk_in, wk), (wval_in, wval), (init_in, init),
+        (wg_in, wg), (tok_in, tok), (wk_in, wk), (wval_in, wval), (wv_in, wv), (wq_in, wq),
+        (extra_in, extra), (wr_in, wr), (woa_in, woa), (wor_in, wor), (init_in, init),
     )
     loads = [pltpu.make_async_copy(a, b, in_sem.at[i]) for i, (a, b) in enumerate(order_in)]
     for load in loads:
@@ -83,8 +83,10 @@
     for k in range(1, count_h):
         greet((s, (t + 2 * k) % nt))
 
-    for load in loads:
-        load.wait()
+    def need(*refs):
+        for load, (_, b) in zip(loads, order_in):
+            if any(b is r for r in refs):
+                load.wait()
 
     rows, width = tok.shape
     part, half, w = wg.shape[0], wg.shape[0] // 2, RECURRENT_WIDTH
@@ -105,21 +107,6 @@
         gb[s, lo_row : lo_row + half] = jnp.where(zl == 0, first, second)
         pk[lo_row : lo_row + half] = jnp.where(zl == 0, second, first)
 
-    split(wg, 0)
-    split(wv, at_v)
-    split(wr, at_r)
-    split_narrow(wq, at_q)
-    split_narrow(woa, at_a)
-    split(wor, at_o)
-    xs[...] = extra[:, pl.ds(pl.multiple_of((1 - zl) * w, w), w)].astype(BF16)
-
-    normed = rms(tok[...].astype(F32), gain[...]).astype(BF16)
-    nf[zl, t] = normed
-    kvb[zl, t, x, zh] = jnp.concatenate(
-        [dot(normed, wk[...], NT).astype(BF16), dot(normed, wval[...], NT).astype(BF16)], axis=1
-    )
-    pl.semaphore_wait(barrier, count_p + count_h)
-
     class Gather:
         def __init__(self, ref, send, recv):
             self.ref, self.send, self.recv = ref, send, recv
@@ -273,26 +260,45 @@
     def sd_swap(side):
         return swap(3, sd.at[side], sd.at[side], (xmate, t))
 
+    need(wg)
+    split(wg, 0)
+    pl.semaphore_wait(barrier, count_p + count_h)
+    row_out(p, 0).start()
+    columns(0)
+    need(tok)
+    normed = rms(tok[...].astype(F32), gain[...]).astype(BF16)
+    nf[zl, t] = normed
+    need(wk, wval)
+    kvb[zl, t, x, zh] = jnp.concatenate(
+        [dot(normed, wk[...], NT).astype(BF16), dot(normed, wval[...], NT).astype(BF16)], axis=1
+    )
     loop(1, count_z, lambda j: k1_copy(j, zh).start())
     tokens.start()
-    row_out(p, 0).start()
+    need(wv, wq)
+    split(wv, at_v)
+    split_narrow(wq, at_q)
     row_out(p, 1).start()
-    columns(0)
     columns(1)
+    need(extra)
+    xs[...] = extra[:, pl.ds(pl.multiple_of((1 - zl) * w, w), w)].astype(BF16)
     extra_swap().start()
+    need(wr, woa, wor, init)
+    split(wr, at_r)
+    split_narrow(woa, at_a)
+    split(wor, at_o)
+    forward(0, 1)
+    forward(0, 0)
+    forward(0, 2)
     loop(1, count_z, lambda j: k1_copy(j, zh + count_z - j).wait_recv())
     kv_swap(x).start()
     row_out(p, 2).start()
     row_out(p, 3).start()
-    forward(0, 0)
+    tokens.relay_y(0)
+    at_middle(lambda: forward(1, 0))
     kv_swap(1 - x).wait_recv()
     keyvals.start()
     columns(2)
-    tokens.relay_y(0)
     tokens.relay_z()
-    at_middle(lambda: forward(1, 0))
-    forward(0, 1)
-    forward(0, 2)
     forward(1, 1)
     at_end(lambda: forward(1, 0))
     tokens.relay_y(1)
@@ -328,7 +334,7 @@
     rr = lax.broadcasted_iota(jnp.int32, (REC_SPAN, REC_SPAN), 0)
     cc = lax.broadcasted_iota(jnp.int32, (REC_SPAN, REC_SPAN), 1)
     lower = (rr >= cc).astype(F32)
-    running, offsets, befores, weighted = [], [], [], []
+    running, offsets, befores, weighted, grown, shrunk = [], [], [], [], [], []
     for j in (0, 1):
         offset = jnp.zeros((1, w), F32)
         for i in range(spans):
@@ -339,6 +345,8 @@
             offsets.append(offset)
             offset = offset + final
             weighted.append((inflow[r] * jnp.exp(final - run)).astype(BF16))
+            grown.append(jnp.exp(run))
+            shrunk.append((inflow[r] * jnp.exp(-run)).astype(BF16))
         sd[x, j] = jnp.broadcast_to(offset, sd.shape[2:])
     at_end(lambda: forward(2, 1))
     forward(2, 2)
@@ -431,25 +439,41 @@
         hidden.append(rms(blended, again[...]))
     attn_hidden = jnp.concatenate(hidden, axis=0).astype(BF16)
 
+    def raw_term(owner):
+        rows_in = nf[:, :, :, pl.ds(pl.multiple_of(owner * part, part), part)]
+        return dot(rows_in.reshape(2 * block, part), gb[owner, at_r:at_a])
+
+    stepwise = small and part % 128 == 0
+    pieces = (p, sources[1], sources[2], sources[0])
+    if stepwise:
+        raw = raw_term(2 * pieces[0] + x)
+        for q in pieces[1:]:
+            raw = raw + raw_term(2 * q + x)
     join_units()
     forward(3, 2)
-    collect(2)
-    raw = dot(full, weight(at_r)).astype(BF16).astype(F32)
+    if stepwise:
+        for q in pieces:
+            row_in(q, 2).wait_recv()
+            raw = raw + raw_term(2 * q + 1 - x)
+    else:
+        collect(2)
+        raw = dot(full, weight(at_r))
+    raw = raw.astype(BF16).astype(F32)
     rec_query = raw * jax.nn.sigmoid(raw)
     local, lifted = [], []
     for j in (0, 1):
         outs, lifts = [], []
         for i in range(spans):
             r = slice(j * block + i * REC_SPAN, j * block + (i + 1) * REC_SPAN)
-            run = running[j * spans + i]
-            before = befores[j * spans + i]
-            dq = (rec_query[r] * jnp.exp(run)).astype(BF16)
-            within = dot(dq, (inflow[r] * jnp.exp(-run)).astype(BF16), NT) * lower
+            m = j * spans + i
+            decayed = rec_query[r] * grown[m]
+            dq = decayed.astype(BF16)
+            within = dot(dq, shrunk[m], NT) * lower
             o = dot(within.astype(BF16), vals[r])
-            if before is not None:
-                o = o + dot(dq, before.astype(BF16), NT)
+            if befores[m] is not None:
+                o = o + dot(dq, befores[m].astype(BF16), NT)
             outs.append(o)
-            lifts.append(rec_query[r] * jnp.exp(offsets[j * spans + i] + run))
+            lifts.append(decayed * jnp.exp(offsets[m]))
         local.append(jnp.concatenate(outs, axis=0))
         lifted.append(jnp.concatenate(lifts, axis=0).astype(BF16))
 

time: 57.3 us -> 54.2 us (0.946); the launches traced: 57.1 us -> 53.2 us
  Pallas kernels: 55.5 us -> 51.6 us
    pallas_call x1, Pallas kernels: 55.5 us -> 51.6 us  [body(): pl.pallas_call(functools.partial(kernel, n, nt), out_shape=jax.ShapeDtype...]
where the time goes in v3:
time: 54.2 us; the launch traced here: 53.2 us
  Pallas kernels  51.6 us (95%)
  local copies, waits for them, and re-layouts  1.62 us (3%)
    pallas_call x1, Pallas kernels, body(): pl.pallas_call(functools.partial(kernel, n, nt), out_shape=jax.ShapeDtype...  51.6 us
    unnamed x1, local copies, waits for them, and re-layouts  1.62 us

profile of v3, /device:TPU:0, one launch (start us, length us, event | category | flops | bytes accessed | tf_op | source)
XLA Modules:
  0.0 53.2 jit_solution(14399916903689566347)
XLA Ops:
  0.0 51.6 %shard_map.154 = bf16[48,2048]{1,0:T(8,128)(2,1)} custom-call(bf16[48,2048]{1,0:T(8,128)(2,1)} %tok_in.1, f32[1,2048]{1,0:T(1,128)} %bitcast.8, bf16[256,128]{1,0:T(8,128)(2,1)} %wq_in.1, bf16[256,256]{1,0:T(8,128)(2,1)} %wg_in.1, bf16[256,256]{1,0:T(8,128)(2,1)} %wv_in.1, bf16[256,256]{1,0:T(8,128)(2,1)} %wr_in.1, bf16[256,128]{1,0:T(8,128)(2,1)} %woa_in.1, ...), custom_call_target="tpu_custom_call" | custom-call | tf_op jit(solution)/shard_map/pallas_call | solution.py:639
  51.6 1.6 %copy.18 = bf16[48,2048]{1,0:T(8,128)(2,1)} copy(bf16[48,2048]{1,0:T(8,128)(2,1)} %shard_map.154) | data formatting | bytes 393216

commit v4 on v3

--- a/solution.py
+++ b/solution.py
@@ -107,94 +107,125 @@
         gb[s, lo_row : lo_row + half] = jnp.where(zl == 0, first, second)
         pk[lo_row : lo_row + half] = jnp.where(zl == 0, second, first)
 
+    def sent(ref, sem):
+        remote(ref, ref, sem, sem, (xmate, t)).wait_send()
+
     class Gather:
-        def __init__(self, ref, send, recv):
-            self.ref, self.send, self.recv = ref, send, recv
+        def __init__(self, ref, send, recv, planes, extent, first):
+            self.ref, self.send, self.recv, self.planes = ref, send, recv, planes
+            self.pieces = (slice(0, first), slice(first, extent))
 
         def slot(self, zz, owner):
+            if self.planes == 1:
+                return self.ref.at[owner % nt]
             return self.ref.at[zl if zz == 0 else 1 - zl, owner % nt]
 
-        def copy(self, kind, zz, k, owner, device):
+        def sems(self, kind, i):
+            past = (0, self.planes, self.planes + count_h - 1, self.planes + count_h + 1)[kind]
+            return self.send.at[min(kind, 1)], self.recv.at[past + i]
+
+        def copy(self, kind, i, owner, zz, device):
             block = self.slot(zz, owner)
-            return remote(block, block, self.send.at[kind, zz, k], self.recv.at[kind, zz, k], device)
+            return remote(block, block, *self.sems(kind, i), device)
+
+        def blocks(self, count):
+            return self.ref.at[0:count] if self.planes == 1 else self.ref.at[0, 0:count]
 
         def core_out(self, zz, k):
-            return self.copy(0, zz, k, t + nt - 2 * k, (s, cmate))
-
-        def core_in(self, zz, k):
-            return self.copy(0, zz, k, cmate + nt - 2 * k, (s, cmate))
-
-        def y_out(self, zz, k):
-            return self.copy(1, zz, k, t, (s, (t + 2 * k) % nt))
-
-        def y_in(self, zz, k):
-            return self.copy(1, zz, k, t + nt - 2 * k, (s, (t + nt - 2 * k) % nt))
-
-        def z_out(self):
-            return self.copy(2, 0, 0, t, (zmate, t))
-
-        def z_in(self):
-            block = self.slot(1, t)
-            return remote(block, block, self.send.at[2, 0, 0], self.recv.at[2, 0, 0], (zmate, t))
+            return self.copy(0, zz, t + nt - 2 * k, zz, (s, cmate))
+
+        def y_out(self, k):
+            return self.copy(1, k - 1, t, 0, (s, (t + 2 * k) % nt))
+
+        def y_in(self, k):
+            return self.copy(1, k - 1, t + nt - 2 * k, 0, (s, (t + nt - 2 * k) % nt))
+
+        def piece(self, zz, owner, h):
+            return self.slot(zz, owner).at[self.pieces[h]]
+
+        def z_out(self, h):
+            block = self.piece(0, t, h)
+            return remote(block, block, *self.sems(2, h), (zmate, t))
+
+        def z_in(self, h):
+            block = self.piece(1, t, h)
+            return remote(block, block, *self.sems(2, h), (zmate, t))
+
+        def zy_out(self, h, k):
+            block = self.piece(1, t, h)
+            return remote(block, block, *self.sems(3, k - 1), (s, (t + 2 * k) % nt))
+
+        def zy_in(self, k):
+            return self.copy(3, k - 1, t + nt - 2 * k, 1, (s, (t + nt - 2 * k) % nt))
 
         def start(self):
-            self.z_out().start()
             for k in range(1, count_h):
-                self.y_out(0, k).start()
+                self.y_out(k).start()
             self.core_out(0, 0).start()
 
-        def relay_z(self):
-            self.z_in().wait_recv()
+        def start_z(self):
+            for h in (0, 1):
+                self.z_out(h).start()
+
+        def relay_z(self, h):
+            self.z_in(h).wait_recv()
             for k in range(1, count_h):
-                self.y_out(1, k).start()
-            self.core_out(1, 0).start()
-
-        def relay_y(self, zz):
+                self.zy_out(h, k).start()
+            if h == 1:
+                self.core_out(1, 0).start()
+
+        def relay_y(self):
             for k in range(1, count_h):
-                self.y_in(zz, k).wait_recv()
-                self.core_out(zz, k).start()
-
-        def arrive(self):
-            for zz in (0, 1):
-                for k in range(count_h):
-                    self.core_in(zz, k).wait_recv()
+                self.y_in(k).wait_recv()
+                self.core_out(0, k).start()
+
+        def relay_zy(self):
+            for k in range(1, count_h):
+                self.zy_in(k).wait_recv()
+                self.core_out(1, k).start()
+
+        def arrive(self, zz):
+            both = self.blocks(count_h)
+            remote(both, both, *self.sems(0, zz), (s, cmate)).wait_recv()
 
         def finish(self):
-            self.z_out().wait_send()
-            for zz in (0, 1):
-                for k in range(count_h):
-                    self.core_out(zz, k).wait_send()
-                    if k > 0:
-                        self.y_out(zz, k).wait_send()
-
-    tokens, keyvals = Gather(nf, tg_send, tg_recv), Gather(kvb, kg_send, kg_recv)
-
-    def cut(ref, g):
-        return ref.at[groups[g][0] : groups[g][1]]
+            if self.planes == 1:
+                sent(self.blocks(count_h), self.send.at[0])
+                sent(self.blocks(count_h - 1), self.send.at[1])
+            else:
+                sent(self.blocks(nt), self.send.at[0])
+                sent(self.blocks(nt - 1), self.send.at[1])
+
+    tokens = Gather(nf, tg_send, tg_recv, 2, rows, (rows // 2 + 15) // 16 * 16)
+    keyvals = Gather(kvb, kg_send, kg_recv, 1, 0, 0)
+
+    def cut(ref, g, many=False):
+        rows_of = slice(groups[g][0], groups[g][1])
+        return ref.at[:, rows_of] if many else ref.at[rows_of]
 
     def col_out(p2, g, same):
         return remote(
             cut(gb.at[s], g) if same else cut(pk, g), cut(gb.at[s], g),
-            col_send.at[p2, g], col_recv.at[p, g], (2 * p2 + x, t),
+            col_send.at[0], col_recv.at[p, g], (2 * p2 + x, t),
         )
 
     def col_in(p2, g):
         slot = cut(gb.at[2 * p2 + x], g)
-        return remote(slot, slot, col_send.at[p2, g], col_recv.at[p2, g], (2 * p2 + x, t))
+        return remote(slot, slot, col_send.at[0], col_recv.at[p2, g], (2 * p2 + x, t))
 
     def row_out(p2, g):
         slot = cut(gb.at[2 * p2 + x], g)
-        return remote(slot, slot, row_send.at[p2, g], row_recv.at[p2, g], (xmate, t))
+        return remote(slot, slot, row_send.at[0], row_recv.at[g if g < 2 else 2 + (g - 2) * count_p + p2], (xmate, t))
 
     def row_in(p2, g):
         slot = cut(gb.at[2 * p2 + 1 - x], g)
-        return remote(slot, slot, row_send.at[p2, g], row_recv.at[p2, g], (xmate, t))
-
-    def near(d, body):
+        return remote(slot, slot, row_send.at[0], row_recv.at[g if g < 2 else 2 + (g - 2) * count_p + p2], (xmate, t))
+
+    def near(d, body, skip=-1):
         for sign in (1, -1):
             p2 = p + sign * d
 
-            @pl.when((p2 >= 0) & (p2 < count_p))
+            @pl.when((p2 >= 0) & (p2 < count_p) & (p2 != skip))
             def _():
                 body(p2)
 
@@ -206,8 +237,32 @@
             loop(0, count_p // 2, lambda i: body(2 * i + 1, False))
             loop(1, count_p // 2, lambda i: body(2 * i, True))
 
+    at_edge = (p == 0) | (p == count_p - 1)
+
+    def at_end(body):
+        if small:
+            pl.when(at_edge)(body)
+
+    def at_middle(body):
+        if small:
+            pl.when(jnp.logical_not(at_edge))(body)
+        else:
+            body()
+
+    def to_mate(g):
+        if small:
+            col_out(p + 1 - 2 * zl, g, False).start()
+
+    def to_rest(g):
+        if small:
+            for d in range(1, count_p):
+                near(d, lambda p2: col_out(p2, g, d % 2 == 0).start(), p + 1 - 2 * zl)
+        else:
+            distances(lambda d, same: near(d, lambda p2: col_out(p2, g, same).start()))
+
     def columns(g):
-        distances(lambda d, same: near(d, lambda p2: col_out(p2, g, same).start()))
+        to_mate(g)
+        to_rest(g)
 
     sources = (count_z - zh, p + 1 - 2 * zl, (count_p - 1) * (1 - zh))
 
@@ -221,35 +276,23 @@
         elif i == 0:
             loop(1, count_p, lambda e: near(e, lambda p2: forward_one(g, p2)))
 
-    at_edge = (p == 0) | (p == count_p - 1)
-
-    def at_end(body):
-        if small:
-            pl.when(at_edge)(body)
-
-    def at_middle(body):
-        if small:
-            pl.when(jnp.logical_not(at_edge))(body)
+    def collect(g):
+        if g < 2:
+            column = cut(gb.at[0:count_p], g, True)
+            remote(column, column, row_send.at[0], row_recv.at[g], (xmate, t)).wait_recv()
         else:
-            body()
-
-    def collect(g):
-        loop(0, count_p, lambda p2: row_in(p2, g).wait_recv())
-
-    def finish(g):
-        distances(lambda d, same: near(d, lambda p2: col_out(p2, g, same).wait_send()))
-        loop(0, count_p, lambda p2: row_out(p2, g).wait_send())
+            loop(0, count_p, lambda p2: row_in(p2, g).wait_recv())
 
     def k1_copy(j, owner):
-        block = kvb.at[zl, t, x, owner % count_z]
-        peer = (zh + j) % count_z
-        return remote(block, block, k1_send.at[j], k1_recv.at[j], (4 * peer + 2 * zl + x, t))
+        block = kvb.at[t, x, owner % count_p]
+        peer = (p + j) % count_p
+        return remote(block, block, k1_send.at[0], k1_recv.at[0], (2 * peer + x, t))
 
     def swap(i, src, dst, device):
         return remote(src, dst, x_send.at[i], x_recv.at[i], device)
 
     def kv_swap(side):
-        return swap(0, kvb.at[zl, t, side], kvb.at[zl, t, side], (xmate, t))
+        return swap(0, kvb.at[t, side], kvb.at[t, side], (xmate, t))
 
     def extra_swap():
         return swap(1, xs, xb, (zmate, t))
@@ -264,21 +307,30 @@
     split(wg, 0)
     pl.semaphore_wait(barrier, count_p + count_h)
     row_out(p, 0).start()
-    columns(0)
+    to_mate(0)
+    at_middle(lambda: to_rest(0))
     need(tok)
     normed = rms(tok[...].astype(F32), gain[...]).astype(BF16)
     nf[zl, t] = normed
     need(wk, wval)
-    kvb[zl, t, x, zh] = jnp.concatenate(
+    kvb[t, x, p] = jnp.concatenate(
         [dot(normed, wk[...], NT).astype(BF16), dot(normed, wval[...], NT).astype(BF16)], axis=1
     )
-    loop(1, count_z, lambda j: k1_copy(j, zh).start())
+    loop(1, count_p, lambda j: k1_copy(j, p).start())
     tokens.start()
     need(wv, wq)
     split(wv, at_v)
     split_narrow(wq, at_q)
     row_out(p, 1).start()
-    columns(1)
+    to_mate(1)
+    at_middle(lambda: to_rest(1))
+    tokens.start_z()
+
+    def far():
+        to_rest(0)
+        to_rest(1)
+
+    at_end(far)
     need(extra)
     xs[...] = extra[:, pl.ds(pl.multiple_of((1 - zl) * w, w), w)].astype(BF16)
     extra_swap().start()
@@ -288,27 +340,38 @@
     split(wor, at_o)
     forward(0, 1)
     forward(0, 0)
-    forward(0, 2)
-    loop(1, count_z, lambda j: k1_copy(j, zh + count_z - j).wait_recv())
+    others = kvb.at[0, 0, 0 : count_p - 1]
+    remote(others, others, k1_send.at[0], k1_recv.at[0], (xmate, t)).wait_recv()
     kv_swap(x).start()
     row_out(p, 2).start()
+    tokens.relay_y()
+    forward(1, 1)
+    forward(1, 0)
     row_out(p, 3).start()
-    tokens.relay_y(0)
-    at_middle(lambda: forward(1, 0))
     kv_swap(1 - x).wait_recv()
     keyvals.start()
     columns(2)
-    tokens.relay_z()
-    forward(1, 1)
-    at_end(lambda: forward(1, 0))
-    tokens.relay_y(1)
+    tokens.relay_z(0)
+    forward(0, 2)
+    tokens.relay_z(1)
     forward(1, 2)
     columns(3)
-    keyvals.relay_z()
-    keyvals.relay_y(0)
+    keyvals.relay_y()
+    tokens.relay_zy()
     at_middle(lambda: forward(2, 0))
     at_middle(lambda: forward(2, 1))
-    tokens.arrive()
+    at_end(lambda: forward(2, 1))
+
+    def on_core(c, body):
+        pl.when(lo == c)(body)
+
+    def last_two():
+        forward(2, 2)
+        forward(2, 0)
+
+    at_end(lambda: on_core(1, last_two))
+    tokens.arrive(0)
+    tokens.arrive(1)
     extra_swap().wait_recv()
     collect(0)
 
@@ -348,9 +411,8 @@
             grown.append(jnp.exp(run))
             shrunk.append((inflow[r] * jnp.exp(-run)).astype(BF16))
         sd[x, j] = jnp.broadcast_to(offset, sd.shape[2:])
-    at_end(lambda: forward(2, 1))
-    forward(2, 2)
-    at_end(lambda: forward(2, 0))
+    at_middle(lambda: forward(2, 2))
+    at_end(lambda: on_core(0, last_two))
     collect(1)
     both = dot(full, jnp.concatenate([weight(at_v), widen(gb[:, at_q:at_r])], axis=1)).astype(BF16)
     vals, queries = both[:, :w], both[:, w:]
@@ -399,16 +461,15 @@
         for copy in un_pair(z2, zh):
             copy.wait_send()
 
-    keyvals.relay_y(1)
-    keyvals.arrive()
+    keyvals.arrive(0)
 
     forward(3, 1)
-    zs = max(1, min(count_z, KEY_BLOCK // (4 * block)))
-    blocks = count_z // zs
+    zs = max(1, min(count_p, KEY_BLOCK // (2 * block)))
+    blocks = count_p // zs
     scale = math.log2(math.e) / math.sqrt(QK_DIM)
 
     def attend(query, b):
-        both = kvb[:, :, :, pl.ds(b * zs, zs)].reshape(4 * zs * block, kvb.shape[5])
+        both = kvb[:, :, pl.ds(b * zs, zs)].reshape(2 * zs * block, kvb.shape[4])
         values = both[:, 2 * QK_DIM :]
         parts = []
         for comp in range(2):
@@ -500,18 +561,18 @@
     chunks = n // per
 
     def d_copy(ch):
-        return remote(pb.at[ch, 1 - lo], db.at[ch], d_send.at[ch], d_recv.at[ch], (s, cmate))
+        return remote(pb.at[ch, 1 - lo], db.at[ch], d_send.at[0], d_recv.at[ch], (s, cmate))
 
     def y_copy(ch, k, flip):
         h2 = (hi + k) % count_h
         src = zb.at[ch, pl.ds(h2, 1)] if flip else sb.at[ch, pl.ds(2 * h2, 2)]
         dst = yr.at[ch, k, pl.ds(0, 1)] if flip else yr.at[ch, k]
-        return remote(src, dst, y_send.at[ch, k], y_recv.at[ch, k], (s, 2 * h2 + lo))
+        return remote(src, dst, y_send.at[int(flip)], y_recv.at[ch, k - 1], (s, 2 * h2 + lo))
 
     def z_copy(ch, flip):
         src = sb.at[ch, pl.ds(count_h * (1 - zl), count_h)] if flip else zb.at[ch, pl.ds(1 - zl, 1)]
         dst = zr.at[ch] if flip else zr.at[ch, pl.ds(0, 1)]
-        return remote(src, dst, z_send.at[ch], z_recv.at[ch], (zmate, t))
+        return remote(src, dst, z_send.at[int(flip)], z_recv.at[ch], (zmate, t))
 
     def stage_d(ch):
         shard = gb[pl.ds(ch * per, per)]
@@ -566,7 +627,7 @@
 
     def store(ch):
         cols = pl.ds(pl.multiple_of(ch * fw, fw), fw)
-        return pltpu.make_async_copy(out.at[:, cols], out_ref.at[:, cols], out_sem.at[ch])
+        return pltpu.make_async_copy(out.at[:, cols], out_ref.at[:, cols], out_sem.at[0])
 
     if small and per == 1:
         order = [(q, c) for c in (0, 1) for q in (2 * zh, 2 * zh + 1)]
@@ -589,23 +650,25 @@
             if 0 <= i - late < lag:
                 body(ready[i - late][0], (i - late) % 2 == 1)
 
-    for g in (0, 1, 2, 3):
-        finish(g)
+    sent(gb.at[0 : count_p - 1], col_send.at[0])
+    sent(gb.at[0:count_p], row_send.at[0])
     tokens.finish()
     keyvals.finish()
-    loop(1, count_z, lambda j: k1_copy(j, zh).wait_send())
+    sent(others, k1_send.at[0])
     kv_swap(x).wait_send()
     extra_swap().wait_send()
     st_swap(x).wait_send()
     sd_swap(x).wait_send()
     loop(zh + 1, count_z, un_done)
 
-    for i, (ch, _) in enumerate(ready):
-        d_copy(ch).wait_send()
-        for k in range(1, count_h):
-            y_copy(ch, k, i % 2 == 1).wait_send()
-        z_copy(ch, i % 2 == 1).wait_send()
-        store(ch).wait()
+    odd = chunks // 2
+    even = chunks - odd
+    sent(yr.at[0:even, 0 : count_h - 1], y_send.at[0])
+    sent(zb.at[0:even, 0:1], z_send.at[0])
+    sent(zb.at[0:odd, 0 : count_h - 1], y_send.at[1])
+    sent(zb.at[0:odd, 0:count_h], z_send.at[1])
+    sent(db, d_send.at[0])
+    pltpu.make_async_copy(out, out_ref, out_sem.at[0]).wait()
 
 
 def solution(mesh):
@@ -643,11 +706,11 @@
             out_specs=hb,
             scratch_shapes=[pltpu.VMEM(a.shape, a.dtype) for a in staged] + [
                 pltpu.VMEM((rows, width), BF16),
-                dma((len(staged),)), dma((chunks,)),
+                dma((len(staged),)), dma((1,)),
                 pltpu.VMEM((n, 5 * part, w), BF16),
                 pltpu.VMEM((5 * part, w), BF16),
                 pltpu.VMEM((2, nt, rows, width), BF16),
-                pltpu.VMEM((2, nt, 2, count_z, rows, kv_width), BF16),
+                pltpu.VMEM((nt, 2, count_p, rows, kv_width), BF16),
                 pltpu.VMEM((span, w), BF16),
                 pltpu.VMEM((span, w), BF16),
                 pltpu.VMEM((2, 2, w, w), BF16),
@@ -660,17 +723,17 @@
                 pltpu.VMEM((chunks, count_h, 2, rows, fw), BF16),
                 pltpu.VMEM((chunks, max(2, count_h), rows, fw), BF16),
                 pltpu.VMEM((chunks, max(2, count_h), rows, fw), BF16),
-                dma((count_p, 4)), dma((count_p, 4)),
-                dma((count_p, 4)), dma((count_p, 4)),
-                dma((3, 2, count_h)), dma((3, 2, count_h)),
-                dma((3, 2, count_h)), dma((3, 2, count_h)),
-                dma((count_z,)), dma((count_z,)),
+                dma((1,)), dma((count_p, 4)),
+                dma((1,)), dma((2 + 2 * count_p,)),
+                dma((2,)), dma((2 * count_h + 2,)),
+                dma((2,)), dma((count_h,)),
+                dma((1,)), dma((1,)),
                 dma((4,)), dma((4,)),
                 dma((count_z,)), dma((count_z,)),
                 dma((count_z,)), dma((count_z,)),
-                dma((chunks,)), dma((chunks,)),
-                dma((chunks, count_h)), dma((chunks, count_h)),
-                dma((chunks,)), dma((chunks,)),
+                dma((1,)), dma((chunks,)),
+                dma((2,)), dma((chunks, count_h - 1)),
+                dma((2,)), dma((chunks,)),
             ],
             compiler_params=pltpu.CompilerParams(
                 has_side_effects=True, collective_id=0, vmem_limit_bytes=60 * 1024 * 1024

time: 54.2 us -> 52.5 us (0.969); the launches traced: 53.2 us -> 52.1 us
  Pallas kernels: 51.6 us -> 50.5 us
    pallas_call x1, Pallas kernels: 51.6 us -> 50.5 us  [body(): pl.pallas_call(functools.partial(kernel, n, nt), out_shape=jax.ShapeDtype...]
where the time goes in v4:
time: 52.5 us; the launch traced here: 52.1 us
  Pallas kernels  50.5 us (96%)
  local copies, waits for them, and re-layouts  1.62 us (3%)
    pallas_call x1, Pallas kernels, body(): pl.pallas_call(functools.partial(kernel, n, nt), out_shape=jax.ShapeDtype...  50.5 us
    unnamed x1, local copies, waits for them, and re-layouts  1.62 us

profile of v4, /device:TPU:0, one launch (start us, length us, event | category | flops | bytes accessed | tf_op | source)
XLA Modules:
  0.0 52.1 jit_solution(2793854530804776287)
XLA Ops:
  0.0 50.5 %shard_map.154 = bf16[48,2048]{1,0:T(8,128)(2,1)} custom-call(bf16[48,2048]{1,0:T(8,128)(2,1)} %tok_in.1, f32[1,2048]{1,0:T(1,128)} %bitcast.8, bf16[256,128]{1,0:T(8,128)(2,1)} %wq_in.1, bf16[256,256]{1,0:T(8,128)(2,1)} %wg_in.1, bf16[256,256]{1,0:T(8,128)(2,1)} %wv_in.1, bf16[256,256]{1,0:T(8,128)(2,1)} %wr_in.1, bf16[256,128]{1,0:T(8,128)(2,1)} %woa_in.1, ...), custom_call_target="tpu_custom_call" | custom-call | tf_op jit(solution)/shard_map/pallas_call | solution.py:702
  50.5 1.6 %copy.18 = bf16[48,2048]{1,0:T(8,128)(2,1)} copy(bf16[48,2048]{1,0:T(8,128)(2,1)} %shard_map.154) | data formatting | bytes 393216

commit v5 on v4

--- a/solution.py
+++ b/solution.py
@@ -14,7 +14,7 @@
 REC_SPAN = 64
 KEY_BLOCK = 1536
 OUT_WIDTH = 256
-LAGS = (2, 8, 14)
+LAGS = (2, 9, 15)
 EPS = 1e-06
 MESH = pl.DeviceIdType.MESH
 F32, BF16 = jnp.float32, jnp.bfloat16
@@ -42,10 +42,11 @@
 
 def kernel(
     n, nt,
-    tok_in, gain, wq_in, wg_in, wv_in, wr_in, woa_in, wor_in, wk_in, wval_in, again, rgain, mapw, leak,
-    extra_in, init_in,
+    tok_in, gain_in, wq_in, wg_in, wv_in, wr_in, woa_in, wor_in, wk_in, wval_in, again_in, rgain_in,
+    mapw_in, leak_in, extra_in, init_in,
     out_ref,
-    tok, wq, wg, wv, wr, woa, wor, wk, wval, extra, init, out, in_sem, out_sem,
+    tok, gain, wq, wg, wv, wr, woa, wor, wk, wval, again, rgain, mapw, leak, extra, init, out,
+    in_sem, out_sem,
     gb, pk, nf, kvb, xb, xs, st, sd, un, ud, pb, db, sb, yr, zb, zr,
     col_send, col_recv, row_send, row_recv, tg_send, tg_recv, kg_send, kg_recv,
     k1_send, k1_recv, x_send, x_recv, un_send, un_recv, ud_send, ud_recv,
@@ -65,13 +66,6 @@
             device_id=device, device_id_type=MESH,
         )
 
-    order_in = (
-        (wg_in, wg), (tok_in, tok), (wk_in, wk), (wval_in, wval), (wv_in, wv), (wq_in, wq),
-        (extra_in, extra), (wr_in, wr), (woa_in, woa), (wor_in, wor), (init_in, init),
-    )
-    loads = [pltpu.make_async_copy(a, b, in_sem.at[i]) for i, (a, b) in enumerate(order_in)]
-    for load in loads:
-        load.start()
     barrier = pltpu.get_barrier_semaphore()
 
     def greet(peer):
@@ -82,6 +76,15 @@
     greet((s, cmate))
     for k in range(1, count_h):
         greet((s, (t + 2 * k) % nt))
+
+    order_in = (
+        (wg_in, wg), (tok_in, tok), (gain_in, gain), (wk_in, wk), (wval_in, wval), (wv_in, wv),
+        (wq_in, wq), (extra_in, extra), (wr_in, wr), (woa_in, woa), (wor_in, wor), (init_in, init),
+        (again_in, again), (rgain_in, rgain), (mapw_in, mapw), (leak_in, leak),
+    )
+    loads = [pltpu.make_async_copy(a, b, in_sem.at[i]) for i, (a, b) in enumerate(order_in)]
+    for load in loads:
+        load.start()
 
     def need(*refs):
         for load, (_, b) in zip(loads, order_in):
@@ -237,6 +240,9 @@
             loop(0, count_p // 2, lambda i: body(2 * i + 1, False))
             loop(1, count_p // 2, lambda i: body(2 * i, True))
 
+    def on_core(c, body):
+        pl.when(lo == c)(body)
+
     at_edge = (p == 0) | (p == count_p - 1)
 
     def at_end(body):
@@ -309,7 +315,7 @@
     row_out(p, 0).start()
     to_mate(0)
     at_middle(lambda: to_rest(0))
-    need(tok)
+    need(tok, gain)
     normed = rms(tok[...].astype(F32), gain[...]).astype(BF16)
     nf[zl, t] = normed
     need(wk, wval)
@@ -334,7 +340,7 @@
     need(extra)
     xs[...] = extra[:, pl.ds(pl.multiple_of((1 - zl) * w, w), w)].astype(BF16)
     extra_swap().start()
-    need(wr, woa, wor, init)
+    need(wr, woa, wor, init, again, rgain, mapw, leak)
     split(wr, at_r)
     split_narrow(woa, at_a)
     split(wor, at_o)
@@ -360,10 +366,7 @@
     tokens.relay_zy()
     at_middle(lambda: forward(2, 0))
     at_middle(lambda: forward(2, 1))
-    at_end(lambda: forward(2, 1))
-
-    def on_core(c, body):
-        pl.when(lo == c)(body)
+    at_end(lambda: on_core(1, lambda: forward(2, 1)))
 
     def last_two():
         forward(2, 2)
@@ -411,8 +414,8 @@
             grown.append(jnp.exp(run))
             shrunk.append((inflow[r] * jnp.exp(-run)).astype(BF16))
         sd[x, j] = jnp.broadcast_to(offset, sd.shape[2:])
+    at_end(lambda: on_core(0, lambda: forward(2, 1)))
     at_middle(lambda: forward(2, 2))
-    at_end(lambda: on_core(0, last_two))
     collect(1)
     both = dot(full, jnp.concatenate([weight(at_v), widen(gb[:, at_q:at_r])], axis=1)).astype(BF16)
     vals, queries = both[:, :w], both[:, w:]
@@ -427,6 +430,7 @@
         st[x, j] = carried.astype(BF16)
     st_swap(x).start()
     sd_swap(x).start()
+    at_end(lambda: on_core(0, last_two))
 
 
     def advance(carried, sx, j):
@@ -463,7 +467,6 @@
 
     keyvals.arrive(0)
 
-    forward(3, 1)
     zs = max(1, min(count_p, KEY_BLOCK // (2 * block)))
     blocks = count_p // zs
     scale = math.log2(math.e) / math.sqrt(QK_DIM)
@@ -490,13 +493,14 @@
             parts += [peak, ta * ea + tc * ec, wa * ea + wc * ec]
         return tuple(parts)
 
+    mine = jnp.where(zl == 0, mapw[:, 0:1], mapw[:, 1:2])
     hidden = []
     for j in (0, 1):
         query = queries[j * block : (j + 1) * block]
         got = attend(query, 0)
         if blocks > 1:
             got = lax.fori_loop(1, blocks, lambda b, g: merge(g, attend(query, b)), got)
-        blended = got[2] / got[1] - mapw[zl] * (got[5] / got[4])
+        blended = got[2] / got[1] - mine * (got[5] / got[4])
         hidden.append(rms(blended, again[...]))
     attn_hidden = jnp.concatenate(hidden, axis=0).astype(BF16)
 
@@ -504,6 +508,7 @@
         rows_in = nf[:, :, :, pl.ds(pl.multiple_of(owner * part, part), part)]
         return dot(rows_in.reshape(2 * block, part), gb[owner, at_r:at_a])
 
+    forward(3, 1)
     stepwise = small and part % 128 == 0
     pieces = (p, sources[1], sources[2], sources[0])
     if stepwise:
@@ -693,16 +698,18 @@
         chunks = width // fw
         kv_width = 2 * QK_DIM + HEAD_DIM
         wk, wval = shared_key_weight.T, shared_value_weight.T
-        staged = (tokens, *weights, wk, wval, extra_log_decay, initial_recurrent_state)
+        staged = (
+            tokens, input_norm_gain[None], *weights, wk, wval, attention_head_gain[None],
+            recurrent_head_gain[None], second_map_weight[None], forget_leak_rate[None],
+            extra_log_decay, initial_recurrent_state,
+        )
         hb = pl.BlockSpec(memory_space=pl.ANY)
-        vm = pl.BlockSpec(memory_space=pltpu.VMEM)
-        sm = pl.BlockSpec(memory_space=pltpu.SMEM)
         dma = pltpu.SemaphoreType.DMA
         w = RECURRENT_WIDTH
         return pl.pallas_call(
             functools.partial(kernel, n, nt),
             out_shape=jax.ShapeDtypeStruct((rows, width), BF16),
-            in_specs=[hb, vm] + [hb] * 8 + [vm] * 2 + [sm, vm, hb, hb],
+            in_specs=[hb] * len(staged),
             out_specs=hb,
             scratch_shapes=[pltpu.VMEM(a.shape, a.dtype) for a in staged] + [
                 pltpu.VMEM((rows, width), BF16),
@@ -738,11 +745,7 @@
             compiler_params=pltpu.CompilerParams(
                 has_side_effects=True, collective_id=0, vmem_limit_bytes=60 * 1024 * 1024
             ),
-        )(
-            tokens, input_norm_gain[None], *weights, wk, wval,
-            attention_head_gain[None], recurrent_head_gain[None], second_map_weight,
-            forget_leak_rate[None], extra_log_decay, initial_recurrent_state,
-        )
+        )(*staged)
 
     placed = (
         P(("sp", "tp"), None), P(), P("sp", "tp"), P(), P(), P("sp", "tp"), P("sp", "tp"),

time: 52.5 us -> 51.3 us (0.977)
  Pallas kernels: 50.5 us -> 49.6 us
    pallas_call x1, Pallas kernels: 50.5 us -> 49.6 us  [body(): pl.pallas_call(functools.partial(kernel, n, nt), out_shape=jax.ShapeDtype...]
where the time goes in v5:
time: 51.3 us; the launch traced here: 51.2 us
  Pallas kernels  49.6 us (97%)
  local copies, waits for them, and re-layouts  1.62 us (3%)
    pallas_call x1, Pallas kernels, body(): pl.pallas_call(functools.partial(kernel, n, nt), out_shape=jax.ShapeDtype...  49.6 us
    unnamed x1, local copies, waits for them, and re-layouts  1.62 us

profile of v5, /device:TPU:0, one launch (start us, length us, event | category | flops | bytes accessed | tf_op | source)
XLA Modules:
  0.0 51.2 jit_solution(10297631738418318266)
XLA Ops:
  0.0 49.6 %shard_map.154 = bf16[48,2048]{1,0:T(8,128)(2,1)} custom-call(bf16[48,2048]{1,0:T(8,128)(2,1)} %tok_in.1, f32[1,2048]{1,0:T(1,128)} %bitcast.9, bf16[256,128]{1,0:T(8,128)(2,1)} %wq_in.1, bf16[256,256]{1,0:T(8,128)(2,1)} %wg_in.1, bf16[256,256]{1,0:T(8,128)(2,1)} %wv_in.1, bf16[256,256]{1,0:T(8,128)(2,1)} %wr_in.1, bf16[256,128]{1,0:T(8,128)(2,1)} %woa_in.1, ...), custom_call_target="tpu_custom_call" | custom-call | tf_op jit(solution)/shard_map/pallas_call | solution.py:709
  49.6 1.6 %copy.18 = bf16[48,2048]{1,0:T(8,128)(2,1)} copy(bf16[48,2048]{1,0:T(8,128)(2,1)} %shard_map.154) | data formatting | bytes 393216
